TPU v7x, 512 devices: a whole 4x4x16 slice. The times are simulated.
512 devices in a mesh: kv: 16 (over y, x), tp: 32 (over z, core).
Axes of the slice: x: 4, y: 4, z: 16, core: 2. Of those that a mesh axis runs over, the one named last changes fastest.
Arguments:
- resid: bfloat16 [128, 4096], P('tp', 'kv'), may hold values from -35 to 35
- attn_gain: bfloat16 [4096], replicated, may hold values from 0.099609375 to 1.8984375
- w_query_nope: bfloat16 [4096, 8192], P('kv', 'tp'), may hold values from -0.09375 to 0.09375
- w_query_rope: bfloat16 [4096, 4096], P('kv', 'tp'), may hold values from -0.09375 to 0.09375
- w_latent: bfloat16 [4096, 512], P('kv'), may hold values from -0.09375 to 0.09375
- w_key_rope: bfloat16 [4096, 64], replicated, may hold values from -0.09375 to 0.09375
- latent_gain: bfloat16 [512], replicated, may hold values from 0.099609375 to 1.8984375
- key_up: bfloat16 [512, 64, 128], P(None, 'tp'), may hold values from -0.5 to 0.5
- value_up: bfloat16 [512, 64, 128], P(None, 'tp'), may hold values from -0.25 to 0.25
- w_out: bfloat16 [8192, 4096], P('tp', 'kv'), may hold values from -4 to 4
- post_gain: bfloat16 [4096], replicated, may hold values from 0.099609375 to 1.8984375
- mlp_gain: bfloat16 [4096], replicated, may hold values from 0.099609375 to 1.8984375
- w_gate: bfloat16 [4096, 11008], P('kv', 'tp'), may hold values from -3 to 3
- w_up: bfloat16 [4096, 11008], P('kv', 'tp'), may hold values from -3 to 3
- w_down: bfloat16 [11008, 4096], P('tp', 'kv'), may hold values from -0.0546875 to 0.0546875
- cache_latent: bfloat16 [128, 8192, 512], P('tp', 'kv'), may hold values from -6 to 6
- cache_rope_key: bfloat16 [128, 8192, 64], P('tp', 'kv'), may hold values from -740 to 740
Outputs:
- next_resid: bfloat16 [128, 4096], P('tp', 'kv')
- new_latent: bfloat16 [128, 512], P('tp')
- new_rope_key: bfloat16 [128, 64], P('tp')
All inputs are finite; a program needn't handle non-finite values.
Results may differ from a plain program's by a relative error of at most 0.035.
Values may be sent and summed in bfloat16 or wider, within the bound.
A program may use at most 64 MiB of HBM per device.

v0:
```python
import functools

import jax
import jax.numpy as jnp
from jax import lax
from jax.sharding import Mesh
from jax.sharding import PartitionSpec as P

KV = ("kv_0", "kv_1")


EPS = 1e-06
THETA = 10000.0


def sent_to_all(array, axis):
    size = lax.axis_size(axis)
    return lax.all_to_all(
        jnp.broadcast_to(array[None], (size, *array.shape)), axis, 0, 0, tiled=True
    )


def in_order(tiles, dim):
    shape = list(tiles.shape[1:])
    shape[dim] *= tiles.shape[0]
    return jnp.moveaxis(tiles, 0, dim).reshape(shape)


def collect(array, axis, dim):
    tiles = sent_to_all(array, axis)
    return in_order(tiles, dim)


def of_everyone(array, axis):
    everything = sent_to_all(array, axis)
    return jnp.sum(everything.astype(jnp.float32), axis=0)


def sent_together(arrays, axis, split_dim, concat_dim, along):
    widths = [a.shape[along] for a in arrays]
    both = jnp.concatenate(arrays, axis=along)
    whole = lax.all_to_all(both, axis, split_axis=split_dim, concat_axis=concat_dim, tiled=True)
    return tuple(jnp.split(whole, [sum(widths[:k]) for k in range(1, len(widths))], axis=along))


def over_axes(array, axes):
    return functools.reduce(lax.pmax, axes, array)


def by_axis(array, axes):
    return functools.reduce(lax.psum, axes, array)


def cut_along(array, dim, size):
    shape = array.shape
    tiles = array.reshape(*shape[:dim], size, shape[dim] // size, *shape[dim + 1 :])
    return jnp.moveaxis(tiles, dim, 0)


def summed_on_arrival(array, axis, dim):
    size = lax.axis_size(axis)
    tiles = lax.all_to_all(cut_along(array, dim, size), axis, 0, 0, tiled=True)
    return jnp.sum(tiles.astype(jnp.float32), axis=0)


def sum_packed(arrays, axis, dims):
    size = lax.axis_size(axis)
    tiles = [cut_along(a, dim, size) for a, dim in zip(arrays, dims)]
    lines = jnp.concatenate([b.reshape(size, -1) for b in tiles], axis=1)
    rows = max(16, -(-lines.shape[1] // 1024) * 8)
    lines = jnp.pad(lines, ((0, 0), (0, rows * 128 - lines.shape[1]))).reshape(-1, 128)
    flat, at, finished = (lax.psum_scatter(lines, axis, tiled=True).reshape(-1), 0, [])
    for b in tiles:
        part = b[0]
        finished.append(flat[at : at + part.size].reshape(part.shape))
        at += part.size
    return tuple(finished)


def rotate(vector, position):
    half_width = vector.shape[-1] // 2
    frequency = THETA ** (-jnp.arange(half_width, dtype=jnp.float32) / half_width)
    angles = jnp.asarray(position, jnp.float32) * frequency
    cos_table, sin_table = (jnp.cos(angles), jnp.sin(angles))
    lower_half, upper_half = (vector[..., :half_width], vector[..., half_width:])
    return jnp.concatenate(
        [
            lower_half * cos_table - upper_half * sin_table,
            lower_half * sin_table + upper_half * cos_table,
        ],
        axis=-1,
    )


def body(
    resid,
    attn_gain,
    w_query_nope,
    w_query_rope,
    w_latent,
    w_key_rope,
    latent_gain,
    key_up,
    value_up,
    w_out,
    post_gain,
    mlp_gain,
    w_gate,
    w_up,
    w_down,
    cache_latent,
    cache_rope_key,
):
    kv_count = lax.axis_size(KV)
    kv_index = lax.axis_index(KV)
    tp_index = lax.axis_index("tp")
    own_rows, width_dev = resid.shape
    model_width = width_dev * kv_count
    heads_dev = key_up.shape[1]
    pos_dev = cache_latent.shape[1]
    context = pos_dev * kv_count
    latent_width = cache_latent.shape[2]
    score_scale = (key_up.shape[2] + cache_rope_key.shape[2]) ** (-0.5)
    col_start = kv_index * width_dev
    row_start = tp_index * own_rows

    def block_of(vector):
        return lax.dynamic_slice_in_dim(vector, col_start, width_dev, 0).astype(jnp.float32)[
            None, :
        ]

    gathered = collect(resid, "tp", 0)
    batch_rows = gathered.shape[0]
    gathered_float = gathered.astype(jnp.float32)
    normed_a = (gathered_float * block_of(attn_gain)).astype(jnp.bfloat16)
    own_normed = lax.dynamic_slice_in_dim(normed_a, row_start, own_rows, 0)
    key_rows = lax.dynamic_slice_in_dim(w_key_rope, col_start, width_dev, 0)
    q_nope_sum, q_rope_sum, latent_sum, key_sum, square_sum = (
        of_everyone(
            jnp.dot(normed_a, w_query_nope, preferred_element_type=jnp.float32).astype(
                jnp.bfloat16
            ),
            KV,
        ).astype(jnp.float32),
        of_everyone(
            jnp.dot(normed_a, w_query_rope, preferred_element_type=jnp.float32).astype(
                jnp.bfloat16
            ),
            KV,
        ).astype(jnp.float32),
        of_everyone(
            jnp.dot(own_normed, w_latent, preferred_element_type=jnp.float32).astype(jnp.bfloat16),
            KV,
        ).astype(jnp.float32),
        of_everyone(
            jnp.dot(own_normed, key_rows, preferred_element_type=jnp.float32).astype(jnp.bfloat16),
            KV,
        ).astype(jnp.float32),
        of_everyone(
            jnp.sum(gathered_float * gathered_float, axis=1).astype(jnp.bfloat16), KV
        ).astype(jnp.float32),
    )
    scale_in = lax.rsqrt(square_sum / model_width + EPS)[:, None]
    own_scale = lax.dynamic_slice_in_dim(scale_in, row_start, own_rows, 0)
    q_nope = (q_nope_sum * scale_in).astype(jnp.bfloat16).reshape(batch_rows, heads_dev, -1)
    q_rope = rotate((q_rope_sum * scale_in).reshape(batch_rows, heads_dev, -1), context).astype(
        jnp.bfloat16
    )
    new_latent = (
        latent_sum
        * lax.rsqrt(jnp.mean(latent_sum * latent_sum, axis=1, keepdims=True) + EPS)
        * latent_gain.astype(jnp.float32)[None, :]
    ).astype(jnp.bfloat16)
    new_rope_key = rotate(key_sum * own_scale, context).astype(jnp.bfloat16)
    q_lat = jnp.einsum("bhd,chd->bhc", q_nope, key_up, preferred_element_type=jnp.float32).astype(
        jnp.bfloat16
    )
    seq_lat, seq_rope = sent_together((q_lat, q_rope), "tp", 0, 1, 2)
    scores = (
        jnp.einsum("bhc,bpc->bhp", seq_lat, cache_latent, preferred_element_type=jnp.float32)
        + jnp.einsum("bhr,bpr->bhp", seq_rope, cache_rope_key, preferred_element_type=jnp.float32)
    ) * score_scale
    own_score = (
        jnp.einsum("bhc,bc->bh", seq_lat, new_latent, preferred_element_type=jnp.float32)
        + jnp.einsum("bhr,br->bh", seq_rope, new_rope_key, preferred_element_type=jnp.float32)
    ) * score_scale
    local_peak = jnp.maximum(jnp.max(scores, axis=2), own_score)
    peak = over_axes(local_peak, KV)
    probs = jnp.exp(scores - peak[:, :, None])
    own_prob = jnp.exp(own_score - peak)
    totals = by_axis(jnp.sum(probs, axis=2), KV) + own_prob
    partial_value = jnp.einsum(
        "bhp,bpc->bhc", probs.astype(jnp.bfloat16), cache_latent, preferred_element_type=jnp.float32
    )
    share_width = latent_width // kv_count
    share_start = kv_index * share_width
    own_share = lax.dynamic_slice_in_dim(new_latent, share_start, share_width, 1).astype(
        jnp.float32
    )
    summed = (
        summed_on_arrival(partial_value.astype(jnp.bfloat16), KV, 2)
        + own_prob[:, :, None] * own_share[:, None, :]
    )
    o_lat = (summed / totals[:, :, None]).astype(jnp.bfloat16)
    head_lat = lax.all_to_all(o_lat, "tp", split_axis=1, concat_axis=0, tiled=True)
    up_rows = lax.dynamic_slice_in_dim(value_up, share_start, share_width, 0)
    head_terms = jnp.einsum("bhc,che->bhe", head_lat, up_rows, preferred_element_type=jnp.float32)
    o_heads = (
        of_everyone(head_terms.astype(jnp.bfloat16), KV).astype(jnp.float32).astype(jnp.bfloat16)
    )
    o_flat = o_heads.reshape(batch_rows, -1)
    attended = summed_on_arrival(
        jnp.dot(o_flat, w_out, preferred_element_type=jnp.float32).astype(jnp.bfloat16), "tp", 0
    )
    post_square = by_axis(jnp.sum(attended * attended, axis=1), KV)
    post_part = attended * lax.rsqrt(post_square / model_width + EPS)[:, None] * block_of(post_gain)
    resid_mid = (resid.astype(jnp.float32) + post_part).astype(jnp.bfloat16)
    mid_rows = collect(resid_mid, "tp", 0)
    mid_float = mid_rows.astype(jnp.float32)
    normed_m = (mid_float * block_of(mlp_gain)).astype(jnp.bfloat16)
    gate_part = jnp.dot(normed_m, w_gate, preferred_element_type=jnp.float32)
    up_part = jnp.dot(normed_m, w_up, preferred_element_type=jnp.float32)
    square_part = jnp.sum(mid_float * mid_float, axis=1)
    gate_share, up_share, square_share = tuple(
        (
            part.astype(jnp.float32)
            for part in sum_packed(
                (
                    gate_part.astype(jnp.bfloat16),
                    up_part.astype(jnp.bfloat16),
                    square_part.astype(jnp.bfloat16),
                ),
                KV,
                (0, 0, 0),
            )
        )
    )
    share_scale = lax.rsqrt(square_share / model_width + EPS)[:, None]
    hidden_share = (jax.nn.silu(gate_share * share_scale) * (up_share * share_scale)).astype(
        jnp.bfloat16
    )
    hidden = collect(hidden_share, KV, 0)
    lowered = summed_on_arrival(
        jnp.dot(hidden, w_down, preferred_element_type=jnp.float32).astype(jnp.bfloat16), "tp", 0
    )
    next_resid = (resid_mid.astype(jnp.float32) + lowered).astype(jnp.bfloat16)
    return (next_resid, new_latent, new_rope_key)


def solution(mesh):
    finer = Mesh(mesh.devices.reshape(4, 4, mesh.shape["tp"]), ("kv_0", "kv_1", "tp"))
    placed = (
        P("tp", KV),
        P(),
        P(KV, "tp"),
        P(KV, "tp"),
        P(KV, None),
        P(),
        P(),
        P(None, "tp", None),
        P(None, "tp", None),
        P("tp", KV),
        P(),
        P(),
        P(KV, "tp"),
        P(KV, "tp"),
        P("tp", KV),
        P("tp", KV, None),
        P("tp", KV, None),
    )
    return jax.shard_map(
        body,
        mesh=finer,
        in_specs=placed,
        out_specs=(P("tp", KV), P("tp", None), P("tp", None)),
        check_vma=False,
    )
```

profile of v0, /device:TPU:1, one launch (start us, length us, event | category | flops | bytes accessed | tf_op | source)
XLA Modules:
  0.0 409.7 jit_solution(7705373120690497883)
XLA Ops:
  8.7 16.7 %all-to-all-start = ((bf16[32,4,256]{2,1,0:T(4,128)(2,1)}), bf16[32,4,256]{2,1,0:T(4,128)(2,1)S(1)}, u32[]{:S(2)}, u32[]{:S(2)}) async-start(bf16[32,4,256]{2,1,0:T(4,128)(2,1)} %broadcast_in_dim.18), calls=%async_computation | async-start | bytes 131072 | tf_op jit(solution)/shard_map/all_to_all | solution.py:18
  27.4 11.0 %all-to-all-done = bf16[32,4,256]{2,1,0:T(4,128)(2,1)S(1)} async-done(((bf16[32,4,256]{2,1,0:T(4,128)(2,1)}), bf16[32,4,256]{2,1,0:T(4,128)(2,1)S(1)}, u32[]{:S(2)}, u32[]{:S(2)}) %all-to-all-start) | async-done | bytes 65568 | tf_op jit(solution)/shard_map/all_to_all | solution.py:18
  39.3 6.8 %all-to-all-start.2 = ((bf16[16,1,128]{2,1,0:T(2,128)(2,1)}), bf16[16,1,128]{2,1,0:T(2,128)(2,1)S(1)}, u32[]{:S(2)}, u32[]{:S(2)}) async-start(bf16[16,1,128]{2,1,0:T(2,128)(2,1)} %broadcast_in_dim.20), calls=%async_computation.2 | async-start | bytes 16384 | tf_op jit(solution)/shard_map/all_to_all | solution.py:18
  47.7 4.8 %all-to-all-done.2 = bf16[16,1,128]{2,1,0:T(2,128)(2,1)S(1)} async-done(((bf16[16,1,128]{2,1,0:T(2,128)(2,1)}), bf16[16,1,128]{2,1,0:T(2,128)(2,1)S(1)}, u32[]{:S(2)}, u32[]{:S(2)}) %all-to-all-start.2) | async-done | bytes 4128 | tf_op jit(solution)/shard_map/all_to_all | solution.py:18
  52.5 3.4 all-to-all-start.6
  56.9 5.2 %all-to-all-done.6 = bf16[16,2,128]{2,1,0:T(2,128)(2,1)S(1)} async-done(((bf16[16,2,128]{2,1,0:T(2,128)(2,1)}), bf16[16,2,128]{2,1,0:T(2,128)(2,1)S(1)}, u32[]{:S(2)}, u32[]{:S(2)}) %all-to-all-start.6) | async-done | bytes 8224 | tf_op jit(solution)/shard_map/all_to_all | solution.py:18
  63.0 3.6 all-to-all-start.3
  66.9 8.7 %all-to-all-done.3 = bf16[16,128,128]{2,1,0:T(8,128)(2,1)S(1)} async-done(((bf16[16,128,128]{2,1,0:T(8,128)(2,1)}), bf16[16,128,128]{2,1,0:T(8,128)(2,1)S(1)}, u32[]{:S(2)}, u32[]{:S(2)}) %all-to-all-start.3) | async-done | bytes 524320 | tf_op jit(solution)/shard_map/all_to_all | solution.py:18
  76.8 3.8 all-to-all-start.1
  85.5 7.9 %all-to-all-done.1 = bf16[16,128,256]{2,1,0:T(8,128)(2,1)S(1)} async-done(((bf16[16,128,256]{2,1,0:T(8,128)(2,1)}), bf16[16,128,256]{2,1,0:T(8,128)(2,1)S(1)}, u32[]{:S(2)}, u32[]{:S(2)}) %all-to-all-start.1) | async-done | bytes 1048608 | tf_op jit(solution)/shard_map/all_to_all | solution.py:18
  94.0 4.1 %all-to-all-start.5 = ((bf16[16,4,512]{2,1,0:T(4,128)(2,1)}), bf16[16,4,512]{2,1,0:T(4,128)(2,1)}, u32[]{:S(2)}, u32[]{:S(2)}) async-start(bf16[16,4,512]{2,1,0:T(4,128)(2,1)} %broadcast_in_dim.22), calls=%async_computation.5 | async-start | bytes 131072 | tf_op jit(solution)/shard_map/all_to_all | solution.py:18
  101.4 3.3 all-to-all-done.5
  104.7 10.8 %all-to-all-start.4 = ((bf16[128,2,576]{2,1,0:T(2,128)(2,1)}), bf16[128,2,576]{2,1,0:T(2,128)(2,1)S(1)}, u32[]{:S(2)}, u32[]{:S(2)}) async-start(bf16[128,2,576]{2,1,0:T(2,128)(2,1)} %copy.131), calls=%async_computation.4 | async-start | bytes 655360 | tf_op jit(solution)/shard_map/all_to_all | solution.py:42
  116.8 23.6 %all-to-all-done.4 = bf16[128,2,576]{2,1,0:T(2,128)(2,1)S(1)} async-done(((bf16[128,2,576]{2,1,0:T(2,128)(2,1)}), bf16[128,2,576]{2,1,0:T(2,128)(2,1)S(1)}, u32[]{:S(2)}, u32[]{:S(2)}) %all-to-all-start.4) | async-done | bytes 294944 | tf_op jit(solution)/shard_map/all_to_all | solution.py:42
  142.3 6.8 %pmax.14 = f32[4,64]{1,0:T(4,128)S(1)} all-reduce(f32[4,64]{1,0:T(4,128)S(1)} %fusion.25), channel_id=1, replica_groups=mesh['kv_0'=4,'kv_1'=4,'tp'=32] {'kv_0'}, use_global_device_ids=true, to_apply=%region_8.0 | all-reduce | flops 256 | bytes 2048 | tf_op jit(solution)/shard_map/pmax | solution.py:47
  149.1 6.9 %pmax.15 = f32[4,64]{1,0:T(4,128)S(1)} all-reduce(f32[4,64]{1,0:T(4,128)S(1)} %pmax.14), channel_id=1, replica_groups=mesh['kv_0'=4,'kv_1'=4,'tp'=32] {'kv_1'}, use_global_device_ids=true, to_apply=%region_9.0 | all-reduce | flops 256 | bytes 2048 | tf_op jit(solution)/shard_map/pmax | solution.py:47
  157.7 2.1 reshape.183
  159.8 3.5 all-to-all-start.7
  163.6 8.5 %psum.28 = f32[4,64]{1,0:T(4,128)S(1)} all-reduce(f32[4,64]{1,0:T(4,128)S(1)} %fusion.3), channel_id=1, replica_groups=mesh['kv_0'=4,'kv_1'=4,'tp'=32] {'kv_0'}, use_global_device_ids=true, to_apply=%region_12.0 | all-reduce | flops 256 | bytes 2048 | tf_op jit(solution)/shard_map/psum | solution.py:51
  172.1 8.7 %psum.29 = f32[4,64]{1,0:T(4,128)S(1)} all-reduce(f32[4,64]{1,0:T(4,128)S(1)} %psum.28), channel_id=1, replica_groups=mesh['kv_0'=4,'kv_1'=4,'tp'=32] {'kv_1'}, use_global_device_ids=true, to_apply=%region_13.0 | all-reduce | flops 256 | bytes 2048 | tf_op jit(solution)/shard_map/psum | solution.py:51
  182.2 12.5 %all-to-all-start.8 = ((bf16[32,2,128]{2,1,0:T(2,128)(2,1)}), bf16[32,2,128]{2,1,0:T(2,128)(2,1)S(1)}, u32[]{:S(2)}, u32[]{:S(2)}) async-start(bf16[32,2,128]{2,1,0:T(2,128)(2,1)} %reshape.185), calls=%async_computation.8 | async-start | bytes 32768 | tf_op jit(solution)/shard_map/all_to_all | solution.py:205
  195.4 11.2 %all-to-all-done.8 = bf16[32,2,128]{2,1,0:T(2,128)(2,1)S(1)} async-done(((bf16[32,2,128]{2,1,0:T(2,128)(2,1)}), bf16[32,2,128]{2,1,0:T(2,128)(2,1)S(1)}, u32[]{:S(2)}, u32[]{:S(2)}) %all-to-all-start.8) | async-done | bytes 16416 | tf_op jit(solution)/shard_map/all_to_all | solution.py:205
  207.4 18.9 %all_to_all.97 = bf16[16,128,2,128]{3,1,2,0:T(8,128)(2,1)S(1)} all-to-all(bf16[16,128,2,128]{3,1,2,0:T(8,128)(2,1)S(1)} %broadcast_in_dim.24), channel_id=1, replica_groups=mesh['kv_0'=4,'kv_1'=4,'tp'=32] {'kv_0','kv_1'}, dimensions={0} | all-to-all | bytes 2097152 | tf_op jit(solution)/shard_map/all_to_all | solution.py:18
  226.8 17.7 %all_to_all.98 = bf16[32,4,256]{2,1,0:T(4,128)(2,1)S(1)} all-to-all(bf16[32,4,256]{2,1,0:T(4,128)(2,1)S(1)} %reshape.167), channel_id=1, replica_groups=mesh['kv_0'=4,'kv_1'=4,'tp'=32] {'tp'}, dimensions={0} | all-to-all | bytes 131072 | tf_op jit(solution)/shard_map/all_to_all | solution.py:62
  244.7 6.5 %psum.30 = f32[4]{0:T(128)S(1)} all-reduce(f32[4]{0:T(128)S(1)} %multiply_reduce_fusion.3), channel_id=1, replica_groups=mesh['kv_0'=4,'kv_1'=4,'tp'=32] {'kv_0'}, use_global_device_ids=true, to_apply=%region_17.0 | all-reduce | flops 4 | bytes 32 | tf_op jit(solution)/shard_map/psum | solution.py:51
  252.0 6.6 %psum.31 = f32[4]{0:T(128)S(1)} all-reduce(f32[4]{0:T(128)S(1)} %psum.30), channel_id=1, replica_groups=mesh['kv_0'=4,'kv_1'=4,'tp'=32] {'kv_1'}, use_global_device_ids=true, to_apply=%region_18.0 | all-reduce | flops 4 | bytes 32 | tf_op jit(solution)/shard_map/psum | solution.py:51
  259.3 9.2 %all-to-all-start.11 = ((bf16[32,4,256]{2,1,0:T(4,128)(2,1)}), bf16[32,4,256]{2,1,0:T(4,128)(2,1)S(1)}, u32[]{:S(2)}, u32[]{:S(2)}) async-start(bf16[32,4,256]{2,1,0:T(4,128)(2,1)} %broadcast_in_dim.25), calls=%async_computation.11 | async-start | bytes 131072 | tf_op jit(solution)/shard_map/all_to_all | solution.py:18
  269.3 12.2 %all-to-all-done.11 = bf16[32,4,256]{2,1,0:T(4,128)(2,1)S(1)} async-done(((bf16[32,4,256]{2,1,0:T(4,128)(2,1)}), bf16[32,4,256]{2,1,0:T(4,128)(2,1)S(1)}, u32[]{:S(2)}, u32[]{:S(2)}) %all-to-all-start.11) | async-done | bytes 65568 | tf_op jit(solution)/shard_map/all_to_all | solution.py:18
  284.6 74.4 %reduce-scatter.4.cloned.1.call-done = bf16[48,128]{1,0:T(8,128)(2,1)} async-done(((bf16[768,128]{1,0:T(8,128)(2,1)}), bf16[48,128]{1,0:T(8,128)(2,1)}) %reduce-scatter.4.cloned.1.call-update) | async-done | bytes 12304
  360.9 10.8 %all_to_all.99 = bf16[16,8,344]{2,1,0:T(8,128)(2,1)S(1)} all-to-all(bf16[16,8,344]{2,1,0:T(8,128)(2,1)S(1)} %broadcast_in_dim.26), channel_id=1, replica_groups=mesh['kv_0'=4,'kv_1'=4,'tp'=32] {'kv_0','kv_1'}, dimensions={0} | all-to-all | bytes 176128 | tf_op jit(solution)/shard_map/all_to_all | solution.py:18
  372.5 16.7 %all-to-all-start.13 = ((bf16[32,4,256]{2,1,0:T(4,128)(2,1)}), bf16[32,4,256]{2,1,0:T(4,128)(2,1)S(1)}, u32[]{:S(2)}, u32[]{:S(2)}) async-start(bf16[32,4,256]{2,1,0:T(4,128)(2,1)} %reshape.171), calls=%async_computation.13 | async-start | bytes 131072 | tf_op jit(solution)/shard_map/all_to_all | solution.py:62
  389.9 12.4 %all-to-all-done.13 = bf16[32,4,256]{2,1,0:T(4,128)(2,1)S(1)} async-done(((bf16[32,4,256]{2,1,0:T(4,128)(2,1)}), bf16[32,4,256]{2,1,0:T(4,128)(2,1)S(1)}, u32[]{:S(2)}, u32[]{:S(2)}) %all-to-all-start.13) | async-done | bytes 65568 | tf_op jit(solution)/shard_map/all_to_all | solution.py:62
  (134 shorter events, 35.8 us)
Async XLA Ops:
  7.2 134.1 %copy-start = (bf16[4,512,512]{2,1,0:T(8,128)(2,1)S(1)}, bf16[4,512,512]{2,1,0:T(8,128)(2,1)}, u32[]{:S(2)}) copy-start(bf16[4,512,512]{2,1,0:T(8,128)(2,1)} %param.32) | copy-start | bytes 6291460
  7.2 59.4 %copy-start.7 = (bf16[256,256]{1,0:T(8,128)(2,1)S(1)}, bf16[256,256]{1,0:T(8,128)(2,1)}, u32[]{:S(2)}) copy-start(bf16[256,256]{1,0:T(8,128)(2,1)} %param.19) | copy-start | bytes 393220
  7.2 59.6 %copy-start.2 = (bf16[256,512]{1,0:T(8,128)(2,1)S(1)}, bf16[256,512]{1,0:T(8,128)(2,1)}, u32[]{:S(2)}) copy-start(bf16[256,512]{1,0:T(8,128)(2,1)} %param.21) | copy-start | bytes 786436
  8.7 29.8 %all-to-all-start = ((bf16[32,4,256]{2,1,0:T(4,128)(2,1)}), bf16[32,4,256]{2,1,0:T(4,128)(2,1)S(1)}, u32[]{:S(2)}, u32[]{:S(2)}) async-start(bf16[32,4,256]{2,1,0:T(4,128)(2,1)} %broadcast_in_dim.18), calls=%async_computation | async-start | bytes 131072 | tf_op jit(solution)/shard_map/all_to_all | solution.py:18
  26.7 56.6 %copy-start.11 = (f32[32]{0:T(128)}, f32[32]{0:T(128)S(1)}, u32[]{:S(2)}) copy-start(f32[32]{0:T(128)S(1)} %get-tuple-element.13) | copy-start | bytes 388
  39.3 13.2 %all-to-all-start.2 = ((bf16[16,1,128]{2,1,0:T(2,128)(2,1)}), bf16[16,1,128]{2,1,0:T(2,128)(2,1)S(1)}, u32[]{:S(2)}, u32[]{:S(2)}) async-start(bf16[16,1,128]{2,1,0:T(2,128)(2,1)} %broadcast_in_dim.20), calls=%async_computation.2 | async-start | bytes 16384 | tf_op jit(solution)/shard_map/all_to_all | solution.py:18
  52.5 9.6 %all-to-all-start.6 = ((bf16[16,2,128]{2,1,0:T(2,128)(2,1)}), bf16[16,2,128]{2,1,0:T(2,128)(2,1)S(1)}, u32[]{:S(2)}, u32[]{:S(2)}) async-start(bf16[16,2,128]{2,1,0:T(2,128)(2,1)} %reshape.181), calls=%async_computation.6 | async-start | bytes 16384 | tf_op jit(solution)/shard_map/all_to_all | solution.py:18
  63.0 12.6 %all-to-all-start.3 = ((bf16[16,128,128]{2,1,0:T(8,128)(2,1)}), bf16[16,128,128]{2,1,0:T(8,128)(2,1)S(1)}, u32[]{:S(2)}, u32[]{:S(2)}) async-start(bf16[16,128,128]{2,1,0:T(8,128)(2,1)} %broadcast_in_dim.21), calls=%async_computation.3 | async-start | bytes 1048576 | tf_op jit(solution)/shard_map/all_to_all | solution.py:18
  75.6 1.2 copy-start.1
  76.8 21.6 %copy-start.3 = (bf16[512,2,128]{2,1,0:T(2,128)(2,1)S(1)}, bf16[512,2,128]{2,1,0:T(2,128)(2,1)}, u32[]{:S(2)}) copy-start(bf16[512,2,128]{2,1,0:T(2,128)(2,1)} %param.24) | copy-start | bytes 786436
  76.8 16.6 %all-to-all-start.1 = ((bf16[16,128,256]{2,1,0:T(8,128)(2,1)}), bf16[16,128,256]{2,1,0:T(8,128)(2,1)S(1)}, u32[]{:S(2)}, u32[]{:S(2)}) async-start(bf16[16,128,256]{2,1,0:T(8,128)(2,1)} %broadcast_in_dim.19), calls=%async_computation.1 | async-start | bytes 2097152 | tf_op jit(solution)/shard_map/all_to_all | solution.py:18
  80.6 0.5 copy-start.14
  94.0 10.6 %all-to-all-start.5 = ((bf16[16,4,512]{2,1,0:T(4,128)(2,1)}), bf16[16,4,512]{2,1,0:T(4,128)(2,1)}, u32[]{:S(2)}, u32[]{:S(2)}) async-start(bf16[16,4,512]{2,1,0:T(4,128)(2,1)} %broadcast_in_dim.22), calls=%async_computation.5 | async-start | bytes 131072 | tf_op jit(solution)/shard_map/all_to_all | solution.py:18
  98.3 17.1 %copy-start.12 = (f32[32]{0:T(128)S(1)}, f32[32]{0:T(128)}, u32[]{:S(2)}) copy-start(f32[32]{0:T(128)} %copy-done.11) | copy-start | bytes 388
  98.3 17.1 %copy-start.13 = (f32[32]{0:T(128)S(1)}, f32[32]{0:T(128)}, u32[]{:S(2)}) copy-start(f32[32]{0:T(128)} %get-tuple-element.14) | copy-start | bytes 388
  104.7 35.8 %all-to-all-start.4 = ((bf16[128,2,576]{2,1,0:T(2,128)(2,1)}), bf16[128,2,576]{2,1,0:T(2,128)(2,1)S(1)}, u32[]{:S(2)}, u32[]{:S(2)}) async-start(bf16[128,2,576]{2,1,0:T(2,128)(2,1)} %copy.131), calls=%async_computation.4 | async-start | bytes 655360 | tf_op jit(solution)/shard_map/all_to_all | solution.py:42
  116.7 24.5 %copy-start.10 = (bf16[4,512]{1,0:T(4,128)(2,1)}, bf16[4,512]{1,0:T(4,128)(2,1)S(1)}, u32[]{:S(2)}) copy-start(bf16[4,512]{1,0:T(4,128)(2,1)S(1)} %multiply_convert_fusion.7) | copy-start | bytes 12292
  140.6 1.4 copy-start.4
  159.8 21.0 %all-to-all-start.7 = ((bf16[16,2,4096]{2,1,0:T(2,128)(2,1)}), bf16[16,2,4096]{2,1,0:T(2,128)(2,1)S(1)}, u32[]{:S(2)}, u32[]{:S(2)}) async-start(bf16[16,2,4096]{2,1,0:T(2,128)(2,1)} %reshape.183), calls=%async_computation.7 | async-start | bytes 524288 | tf_op jit(solution)/shard_map/all_to_all | solution.py:62
  182.2 24.4 %all-to-all-start.8 = ((bf16[32,2,128]{2,1,0:T(2,128)(2,1)}), bf16[32,2,128]{2,1,0:T(2,128)(2,1)S(1)}, u32[]{:S(2)}, u32[]{:S(2)}) async-start(bf16[32,2,128]{2,1,0:T(2,128)(2,1)} %reshape.185), calls=%async_computation.8 | async-start | bytes 32768 | tf_op jit(solution)/shard_map/all_to_all | solution.py:205
  207.1 19.4 %copy-start.8 = (bf16[256,256]{1,0:T(8,128)(2,1)S(1)}, bf16[256,256]{1,0:T(8,128)(2,1)}, u32[]{:S(2)}) copy-start(bf16[256,256]{1,0:T(8,128)(2,1)} %param.26) | copy-start | bytes 393220
  207.4 51.2 %copy-start.9 = (bf16[4,256]{1,0:T(4,128)(2,1)S(1)}, bf16[4,256]{1,0:T(4,128)(2,1)}, u32[]{:S(2)}) copy-start(bf16[4,256]{1,0:T(4,128)(2,1)} %param.17) | copy-start | bytes 6148
  207.4 74.4 %copy-start.5 = (bf16[256,344]{0,1:T(8,128)(2,1)S(1)}, bf16[256,344]{0,1:T(8,128)(2,1)}, u32[]{:S(2)}) copy-start(bf16[256,344]{0,1:T(8,128)(2,1)} %param.30) | copy-start | bytes 528388
  226.8 144.9 %copy-start.6 = (bf16[344,256]{1,0:T(8,128)(2,1)S(1)}, bf16[344,256]{1,0:T(8,128)(2,1)}, u32[]{:S(2)}) copy-start(bf16[344,256]{1,0:T(8,128)(2,1)} %param.31) | copy-start | bytes 528388
  259.3 22.2 %all-to-all-start.11 = ((bf16[32,4,256]{2,1,0:T(4,128)(2,1)}), bf16[32,4,256]{2,1,0:T(4,128)(2,1)S(1)}, u32[]{:S(2)}, u32[]{:S(2)}) async-start(bf16[32,4,256]{2,1,0:T(4,128)(2,1)} %broadcast_in_dim.25), calls=%async_computation.11 | async-start | bytes 131072 | tf_op jit(solution)/shard_map/all_to_all | solution.py:18
  268.5 90.5 %reduce-scatter.4.cloned.1.call-start = ((), (), s32[]{:S(2)}) async-start(), calls=%async_computation.15 | async-start | bytes 208896
  372.5 29.7 %all-to-all-start.13 = ((bf16[32,4,256]{2,1,0:T(4,128)(2,1)}), bf16[32,4,256]{2,1,0:T(4,128)(2,1)S(1)}, u32[]{:S(2)}, u32[]{:S(2)}) async-start(bf16[32,4,256]{2,1,0:T(4,128)(2,1)} %reshape.171), calls=%async_computation.13 | async-start | bytes 131072 | tf_op jit(solution)/shard_map/all_to_all | solution.py:62
Sparse Core Ops, SparseCore 0:
  284.8 74.2 reduce-scatter.3
where the time goes:
time: 411 us; the launch traced here: 410 us
  waiting for transfers between devices  175 us (43%)
  blocking collectives  91.5 us (22%)
  starting transfers between devices  91.1 us (22%)
  local copies, waits for them, and re-layouts  18.3 us (4%)
  between operations  14.6 us (4%)
  other arithmetic  12.6 us (3%)
  matrix products  6.91 us (2%)
    unnamed x2, waiting for transfers between devices  74.4 us
    all_to_all x7, waiting for transfers between devices, sent_to_all(): lax.all_to_all(jnp.broadcast_to(array[None], (size, *array.shape)), axis,...  53.1 us
    all_to_all x7, starting transfers between devices, sent_to_all(): lax.all_to_all(jnp.broadcast_to(array[None], (size, *array.shape)), axis,...  47.6 us
    psum x4, blocking collectives, by_axis(): return functools.reduce(lax.psum, axes, array)  30.3 us
    all_to_all x2, blocking collectives, sent_to_all(): lax.all_to_all(jnp.broadcast_to(array[None], (size, *array.shape)), axis,...  29.7 us
    all_to_all x1, waiting for transfers between devices, sent_together(): lax.all_to_all(both, axis, split_axis=split_dim, concat_axis=concat_dim,...  23.6 us
    all_to_all x2, starting transfers between devices, summed_on_arrival(): tiles = lax.all_to_all(cut_along(array, dim, size), axis, 0, 0, tiled=True)  20.2 us
    all_to_all x1, blocking collectives, summed_on_arrival(): tiles = lax.all_to_all(cut_along(array, dim, size), axis, 0, 0, tiled=True)  17.7 us
  transfers between devices with their start and end apart: 12, of which 11 were waited for; matrix products, arithmetic and copies ran while one was open for 4% of the time, Pallas kernels for 0%

commit v1 on v0

v1 whole, which is shorter than its diff:
```python
import functools

import jax
import jax.numpy as jnp
import numpy as np
from jax import lax
from jax.experimental import pallas as pl
from jax.experimental.pallas import tpu as pltpu
from jax.sharding import PartitionSpec as P

EPS = 1e-06
THETA = 10000.0
MESH = pl.DeviceIdType.MESH
F32 = jnp.float32
BF16 = jnp.bfloat16
NN = (((1,), (0,)), ((), ()))
NT = (((1,), (1,)), ((), ()))


def dot(a, b, dims=NN):
    return lax.dot_general(a, b, dims, preferred_element_type=F32)


def halves(value):
    high = value.astype(BF16).astype(F32)
    return high, (value - high).astype(BF16).astype(F32)


def put(ref, rows, value, first=0):
    for c in range(value.shape[1] // 128):
        ref[first + c, rows, :] = value[:, 128 * c : 128 * (c + 1)]


def get(ref, rows):
    return jnp.concatenate([ref[c, rows, :] for c in range(ref.shape[0])], axis=1)


def lanes(shape):
    return lax.broadcasted_iota(jnp.int32, shape, len(shape) - 1)


def rotate(vector, table):
    lower = lanes(vector.shape) % 64 < 32
    partner = jnp.where(lower, pltpu.roll(vector, 96, 1), pltpu.roll(vector, 32, 1))
    return vector * table[0:1, :] + partner * table[1:2, :]


def rotation_table(position):
    frequency = THETA ** (-np.arange(32, dtype=np.float64) / 32)
    angles = position * frequency
    cos, sin = np.cos(angles), np.sin(angles)
    return np.stack(
        [np.tile(np.concatenate([cos, cos]), 2), np.tile(np.concatenate([-sin, sin]), 2)]
    ).astype(np.float32)


INPUTS = (
    "resid",
    "attn_gain",
    "post_gain",
    "mlp_gain",
    "latent_gain",
    "table",
    "wqn",
    "wqr",
    "wl",
    "wkr",
    "ku",
    "vu",
    "wo",
    "wg",
    "wu",
    "wd",
    "cl",
    "cr",
)


def kernel(n_kv, n_tp, *refs):
    n_in = len(INPUTS)
    hbm = dict(zip(INPUTS, refs[:n_in]))
    out_resid, out_latent, out_key = refs[n_in : n_in + 3]
    scratch = refs[n_in + 3 :]
    v = dict(zip(INPUTS, scratch[:n_in]))
    (
        load_sem,
        f1, sb_l, rb_l, rb1, f2, sb2, rb2, f3, sb3, rb3, fq, rb_q, sb4, rb4, f5, sb5, rb5, fo, rb6,
        f7, sb7, rb7, sb8, rb8, mid, rb9, f10, sb10, rb10, sb11, rb11, rb12, sb12, g1, nl,
        tp_send, tp_recv, kv_send, kv_recv, q_recv, o_recv,
    ) = scratch[n_in:]

    k, t = lax.axis_index("kv"), lax.axis_index("tp")
    own = v["resid"].shape[0]
    batch = own * n_tp
    width = v["resid"].shape[1]
    model = width * n_kv
    lat = v["cl"].shape[2]
    quarters = n_kv // own
    share = batch // n_kv
    heads = 2 * n_tp
    heads_q = heads // quarters
    tp_q = n_tp // quarters
    ff = v["wg"].shape[0]
    scale = (v["ku"].shape[2] + 64) ** (-0.5)
    slot, group = lax.rem(k, own), lax.div(k, own)

    loads = {}
    for at, name in enumerate(INPUTS):
        source = hbm[name]
        if name == "wkr":
            source = source.at[:, pl.ds(pl.multiple_of(k * width, width), width)]
        loads[name] = pltpu.make_async_copy(source, v[name], load_sem.at[at])
        loads[name].start()

    barrier = pltpu.get_barrier_semaphore()

    @pl.loop(1, n_tp)
    def _(i):
        pl.semaphore_signal(barrier, inc=1, device_id={"kv": k, "tp": lax.rem(t + i, n_tp)}, device_id_type=MESH)

    @pl.loop(1, n_kv)
    def _(i):
        pl.semaphore_signal(barrier, inc=1, device_id={"kv": lax.rem(k + i, n_kv), "tp": t}, device_id_type=MESH)

    def send(src, dst, send_sem, recv_sem, kv, tp):
        pltpu.make_async_remote_copy(
            src_ref=src,
            dst_ref=dst,
            send_sem=send_sem,
            recv_sem=recv_sem,
            device_id={"kv": kv, "tp": tp},
            device_id_type=MESH,
        ).start()

    def over_tp(src_of, dst, phase):
        @pl.loop(1, n_tp)
        def _(i):
            to = lax.rem(t + i, n_tp)
            send(src_of(to), dst, tp_send.at[phase], tp_recv.at[phase], k, to)

    def over_kv(src_of, dst, phase, recv=None):
        @pl.loop(1, n_kv)
        def _(i):
            to = lax.rem(k + i, n_kv)
            send(src_of(to), dst, kv_send.at[phase], kv_recv.at[phase] if recv is None else recv, to, t)

    def take(ref, sem):
        pltpu.make_async_copy(ref, ref, sem).wait()

    def take_tp(ref, phase):
        take(ref.at[pl.ds(0, n_tp - 1)], tp_recv.at[phase])

    def take_kv(ref, phase):
        take(ref.at[pl.ds(0, n_kv - 1)], kv_recv.at[phase])

    for name in ("attn_gain", "post_gain", "mlp_gain", "resid", "wl", "wkr", "latent_gain", "table"):
        loads[name].wait()

    def block_of(name):
        g1[...] = v[name][...].astype(F32)
        per = width // 128
        return jnp.concatenate([g1[pl.ds(k * per + j, 1), :] for j in range(per)], axis=1)

    attn_gain, post_gain, mlp_gain = block_of("attn_gain"), block_of("post_gain"), block_of("mlp_gain")
    resid = v["resid"][...].astype(F32)
    own_normed = (resid * attn_gain).astype(BF16)
    sb_l[:, 0:lat] = dot(own_normed, v["wl"][...])
    key_part = dot(own_normed, v["wkr"][...], NT)
    square = jnp.sum(resid * resid, axis=1, keepdims=True)
    sb_l[:, lat : lat + 128] = jnp.concatenate([key_part, jnp.broadcast_to(square, (own, 64))], axis=1)

    pl.semaphore_wait(barrier, n_tp + n_kv - 2)

    over_tp(lambda to: v["resid"], rb1.at[t], 0)
    over_kv(lambda to: sb_l, rb_l.at[k], 0)
    rb1[t] = v["resid"][...]
    rb_l[k] = sb_l[...]
    for name in INPUTS:
        if name in ("wqn", "wqr", "ku", "vu", "wo", "wg", "wu", "wd"):
            loads[name].wait()
    take_tp(rb1, 0)
    for j in range(n_tp):
        f1[own * j : own * (j + 1), :] = rb1[j].astype(F32)
    rows = f1[...]
    normed = (rows * attn_gain).astype(BF16)
    high, low = halves(jnp.sum(rows * rows, axis=1, keepdims=True))
    qw = v["wqn"].shape[1]
    every = slice(None)
    put(f2, every, dot(normed, v["wqn"][...]))
    put(f2, every, dot(normed, v["wqr"][...]), qw // 128)
    put(f2, every, jnp.where(lanes((batch, 128)) < 64, high, low), qw // 128 + 1)
    for j in range(n_kv):
        sb2[j] = get(f2, pl.ds(j, share, stride=n_kv)).astype(BF16)
    over_kv(lambda to: sb2.at[to], rb2.at[k], 1)
    rb2[k] = sb2[k]

    take_kv(rb_l, 0)
    total = rb_l[0]
    for j in range(1, n_kv):
        total = total + rb_l[j]
    latent = total[:, 0:lat]
    gain_rows = v["latent_gain"][...].astype(F32)
    latent_gain = jnp.concatenate([gain_rows[j : j + 1, :] for j in range(lat // 128)], axis=1)
    new_latent = (
        latent * lax.rsqrt(jnp.mean(latent * latent, axis=1, keepdims=True) + EPS) * latent_gain
    ).astype(BF16)
    out_latent[...] = new_latent
    key = total[:, lat : lat + 128]
    own_scale = lax.rsqrt(key[:, 64:65] / model + EPS)
    table = v["table"][...]
    new_key = rotate(key * own_scale, table).astype(BF16)
    out_key[...] = new_key[:, 0:64]
    nl[:, 0:lat] = new_latent.astype(F32)
    nl[:, lat : lat + 128] = jnp.where(lanes((own, 128)) < 64, new_key.astype(F32), 0.0)

    take_kv(rb2, 1)
    total = rb2[0].astype(F32)
    for j in range(1, n_kv):
        total = total + rb2[j].astype(F32)
    squares = total[:, qw + 128 : qw + 129] + total[:, qw + 192 : qw + 193]
    scale_in = lax.rsqrt(squares / model + EPS)
    q_nope = (total[:, 0:qw] * scale_in).astype(BF16)
    q_rope = rotate(total[:, qw : qw + 128] * scale_in, table)
    for h in range(2):
        spot = pl.ds(h, share, stride=2)
        put(f3, spot, dot(q_nope[:, 128 * h : 128 * (h + 1)], v["ku"][h], NT))
        turned = q_rope if h == 0 else pltpu.roll(q_rope, 64, 1)
        put(f3, spot, jnp.where(lanes((share, 128)) < 64, turned, 0.0), lat // 128)
    for i in range(share):
        sb3[i] = get(f3, slice(2 * i, 2 * i + 2)).astype(BF16)
    @pl.loop(0, share)
    def _(i):
        to = quarters * i + group

        @pl.when(to != t)
        def _():
            send(sb3.at[i], rb3.at[t], tp_send.at[1], tp_recv.at[1], k, to)

        @pl.when(to == t)
        def _():
            rb3[t] = sb3[i]

    gathers_q = lax.rem(t, quarters) == group

    @pl.when(gathers_q)
    def _():
        take_tp(rb3, 1)
        for j in range(n_tp):
            fq[2 * j : 2 * j + 2, :] = rb3[j].astype(F32)
        rb_q[slot] = fq[...].astype(BF16)
        over_kv(lambda to: rb_q.at[slot], rb_q.at[slot], 2, q_recv.at[slot])

    loads["cl"].wait()
    loads["cr"].wait()
    for s in range(own):
        @pl.when(k != own * lax.rem(t, quarters) + s)
        def _():
            take(rb_q.at[s], q_recv.at[s])

        keys = v["cl"][s]
        scores = (dot(rb_q[s, :, 0:lat], keys, NT) + dot(rb_q[s, :, lat : lat + 64], v["cr"][s])) * scale
        peak_high, peak_low = halves(jnp.max(scores, axis=1, keepdims=True))
        probs = jnp.exp(scores - (peak_high + peak_low))
        sum_high, sum_low = halves(jnp.sum(probs, axis=1, keepdims=True))
        sb4[s, :, 0:lat] = dot(probs.astype(BF16), keys).astype(BF16)
        lane = lanes((heads, 128))
        sb4[s, :, lat : lat + 128] = jnp.where(
            lane < 32, peak_high, jnp.where(lane < 64, peak_low, jnp.where(lane < 96, sum_high, sum_low))
        ).astype(BF16)
        for q in range(quarters):
            to = own * q + s

            @pl.when(k != to)
            def _():
                send(sb4.at[s, pl.ds(heads_q * q, heads_q)], rb4.at[k], kv_send.at[3], kv_recv.at[3], to, t)

            @pl.when(k == to)
            def _():
                rb4[k] = sb4[s, heads_q * q : heads_q * (q + 1), :]

    query = rb_q[slot, pl.ds(pl.multiple_of(group * heads_q, heads_q), heads_q), :].astype(F32)
    mine = nl[pl.ds(slot, 1), :]
    own_score = jnp.sum(query * mine, axis=1, keepdims=True) * scale
    take_kv(rb4, 3)
    peaks, sums = [], []
    top = own_score
    for j in range(n_kv):
        stats = rb4[j, :, lat : lat + 128].astype(F32)
        peaks.append(stats[:, 0:1] + stats[:, 32:33])
        sums.append(stats[:, 64:65] + stats[:, 96:97])
        top = jnp.maximum(top, peaks[-1])
    own_prob = jnp.exp(own_score - top)
    totals = own_prob
    summed = own_prob * mine[:, 0:lat]
    for j in range(n_kv):
        weight = jnp.exp(peaks[j] - top)
        totals = totals + sums[j] * weight
        summed = summed + rb4[j, :, 0:lat].astype(F32) * weight
    f5[...] = summed / totals
    for i in range(tp_q):
        sb5[i] = f5[2 * i : 2 * i + 2, :].astype(BF16)

    @pl.loop(0, tp_q)
    def _(i):
        to = tp_q * group + i

        @pl.when(to != t)
        def _():
            send(sb5.at[i], rb5.at[t], tp_send.at[2], tp_recv.at[2], k, to)

        @pl.when(to == t)
        def _():
            rb5[t] = sb5[i]

    gathers_o = lax.div(t, tp_q) == group

    @pl.when(gathers_o)
    def _():
        take_tp(rb5, 2)
        for j in range(n_tp):
            put(fo, slice(2 * j, 2 * j + 2), rb5[j].astype(F32))
        terms = [dot(get(fo, pl.ds(h, n_tp, stride=2)).astype(BF16), v["vu"][h]).astype(BF16) for h in range(2)]
        rb6[slot] = jnp.concatenate(terms, axis=1)
        over_kv(lambda to: rb6.at[slot], rb6.at[slot], 4, o_recv.at[slot])

    for s in range(own):
        @pl.when(k != own * lax.div(t, tp_q) + s)
        def _():
            take(rb6.at[s], o_recv.at[s])

        put(f7, slice(n_tp * s, n_tp * (s + 1)), dot(rb6[s], v["wo"][...]))
    for j in range(n_tp):
        sb7[j] = get(f7, pl.ds(j, own, stride=n_tp)).astype(BF16)
    over_tp(lambda to: sb7.at[to], rb7.at[t], 3)
    rb7[t] = sb7[t]
    take_tp(rb7, 3)
    attended = jnp.sum(rb7[...].astype(F32), axis=0)
    sb8[...] = jnp.broadcast_to(jnp.sum(attended * attended, axis=1, keepdims=True), sb8.shape)
    over_kv(lambda to: sb8, rb8.at[k], 5)
    rb8[k] = sb8[...]
    take_kv(rb8, 5)
    post_square = jnp.sum(rb8[...], axis=0)[:, 0:1]
    mid[...] = (resid + attended * lax.rsqrt(post_square / model + EPS) * post_gain).astype(BF16)
    over_tp(lambda to: mid, rb9.at[t], 4)
    rb9[t] = mid[...]
    take_tp(rb9, 4)
    for j in range(n_tp):
        f1[own * j : own * (j + 1), :] = rb9[j].astype(F32)
    rows = f1[...]
    normed = (rows * mlp_gain).astype(BF16)
    high, low = halves(jnp.sum(rows * rows, axis=1, keepdims=True))
    padded = -(-ff // 128) * 128
    free = padded - ff
    f10[:, padded - 128 : padded] = jnp.where(lanes((batch, 128)) < 128 - free // 2, high, low)
    f10[:, 2 * padded - 128 : 2 * padded] = jnp.zeros((batch, 128), F32)
    f10[:, 0:ff] = dot(normed, v["wg"][...], NT)
    f10[:, padded : padded + ff] = dot(normed, v["wu"][...], NT)
    for j in range(n_kv):
        sb10[j] = f10[share * j : share * (j + 1), :].astype(BF16)
    over_kv(lambda to: sb10.at[to], rb10.at[k], 6)
    rb10[k] = sb10[k]
    take_kv(rb10, 6)
    total = rb10[0].astype(F32)
    for j in range(1, n_kv):
        total = total + rb10[j].astype(F32)
    squares = total[:, ff : ff + 1] + total[:, padded - 1 : padded]
    scale_mid = lax.rsqrt(squares / model + EPS)
    gate, up = total[:, 0:padded] * scale_mid, total[:, padded : 2 * padded] * scale_mid
    hidden = gate / (1.0 + jnp.exp(-gate)) * up
    sb11[...] = jnp.where(lanes((share, padded)) < ff, hidden, 0.0).astype(BF16)
    over_kv(lambda to: sb11, rb11.at[k], 7)
    rb11[k] = sb11[...]
    take_kv(rb11, 7)
    everything = rb11[...].astype(F32).reshape(batch, padded).astype(BF16)
    f1[...] = dot(everything[:, 0:ff], v["wd"][...])
    for j in range(n_tp):
        sb12[j] = f1[own * j : own * (j + 1), :].astype(BF16)
    over_tp(lambda to: sb12.at[to], rb12.at[t], 5)
    rb12[t] = sb12[t]
    take_tp(rb12, 5)
    out_resid[...] = (mid[...].astype(F32) + jnp.sum(rb12[...].astype(F32), axis=0)).astype(BF16)

    for phase, ref in ((0, rb1), (3, rb7), (4, rb9), (5, rb12)):
        take(ref.at[pl.ds(0, n_tp - 1)], tp_send.at[phase])
    for phase, ref in ((0, rb_l), (1, rb2), (3, rb4), (5, rb8), (6, rb10), (7, rb11)):
        take(ref.at[pl.ds(0, n_kv - 1)], kv_send.at[phase])
    for phase, ref, count, inside in ((1, rb3, share, gathers_q), (2, rb5, tp_q, gathers_o)):
        @pl.when(inside)
        def _():
            take(ref.at[pl.ds(0, count - 1)], tp_send.at[phase])

        @pl.when(jnp.logical_not(inside))
        def _():
            take(ref.at[pl.ds(0, count)], tp_send.at[phase])

    for phase, ref, inside in ((2, rb_q, gathers_q), (4, rb6, gathers_o)):
        @pl.when(inside)
        def _():
            @pl.loop(1, n_kv)
            def _(i):
                take(ref.at[0], kv_send.at[phase])


def body(
    resid, attn_gain, w_query_nope, w_query_rope, w_latent, w_key_rope, latent_gain, key_up, value_up,
    w_out, post_gain, mlp_gain, w_gate, w_up, w_down, cache_latent, cache_rope_key,
):
    n_kv, n_tp = lax.axis_size("kv"), lax.axis_size("tp")
    own, width = resid.shape
    batch, share = own * n_tp, own * n_tp // n_kv
    lat, positions = cache_latent.shape[2], cache_latent.shape[1]
    quarters = n_kv // own
    heads = 2 * n_tp
    heads_q, tp_q = heads // quarters, n_tp // quarters
    ff = w_gate.shape[1]
    padded = -(-ff // 128) * 128
    qw = w_query_nope.shape[1]
    operands = (
        resid,
        attn_gain.reshape(-1, 128),
        post_gain.reshape(-1, 128),
        mlp_gain.reshape(-1, 128),
        latent_gain.reshape(-1, 128),
        jnp.asarray(rotation_table(positions * n_kv)),
        w_query_nope,
        w_query_rope,
        w_latent,
        w_key_rope.T,
        key_up.transpose(1, 0, 2),
        value_up.transpose(1, 0, 2),
        w_out,
        w_gate.T,
        w_up.T,
        w_down,
        cache_latent,
        cache_rope_key.swapaxes(1, 2),
    )
    local = [pltpu.VMEM(o.shape, o.dtype) for o in operands]
    local[9] = pltpu.VMEM((64, width), BF16)
    wide = lat + 128
    dma = pltpu.SemaphoreType.DMA
    scratch = local + [
        dma((len(INPUTS),)),
        pltpu.VMEM((batch, width), F32),
        pltpu.VMEM((own, wide), F32),
        pltpu.VMEM((n_kv, own, wide), F32),
        pltpu.VMEM((n_tp, own, width), BF16),
        pltpu.VMEM((qw // 128 + 2, batch, 128), F32),
        pltpu.VMEM((n_kv, share, qw + 256), BF16),
        pltpu.VMEM((n_kv, share, qw + 256), BF16),
        pltpu.VMEM((wide // 128, 2 * share, 128), F32),
        pltpu.VMEM((share, 2, wide), BF16),
        pltpu.VMEM((n_tp, 2, wide), BF16),
        pltpu.VMEM((heads, wide), F32),
        pltpu.VMEM((own, heads, wide), BF16),
        pltpu.VMEM((own, heads, wide), BF16),
        pltpu.VMEM((n_kv, heads_q, wide), BF16),
        pltpu.VMEM((heads_q, lat), F32),
        pltpu.VMEM((tp_q, 2, lat), BF16),
        pltpu.VMEM((n_tp, 2, lat), BF16),
        pltpu.VMEM((lat // 128, heads, 128), F32),
        pltpu.VMEM((own, n_tp, 256), BF16),
        pltpu.VMEM((width // 128, batch, 128), F32),
        pltpu.VMEM((n_tp, own, width), BF16),
        pltpu.VMEM((n_tp, own, width), BF16),
        pltpu.VMEM((own, 128), F32),
        pltpu.VMEM((n_kv, own, 128), F32),
        pltpu.VMEM((own, width), BF16),
        pltpu.VMEM((n_tp, own, width), BF16),
        pltpu.VMEM((batch, 2 * padded), F32),
        pltpu.VMEM((n_kv, share, 2 * padded), BF16),
        pltpu.VMEM((n_kv, share, 2 * padded), BF16),
        pltpu.VMEM((share, padded), BF16),
        pltpu.VMEM((n_kv, share, padded), BF16),
        pltpu.VMEM((n_tp, own, width), BF16),
        pltpu.VMEM((n_tp, own, width), BF16),
        pltpu.VMEM((attn_gain.shape[0] // 128, 128), F32),
        pltpu.VMEM((own, wide), F32),
        dma((6,)),
        dma((6,)),
        dma((8,)),
        dma((8,)),
        dma((own,)),
        dma((own,)),
    ]
    return pl.pallas_call(
        functools.partial(kernel, n_kv, n_tp),
        out_shape=(
            jax.ShapeDtypeStruct((own, width), BF16),
            jax.ShapeDtypeStruct((own, lat), BF16),
            jax.ShapeDtypeStruct((own, 64), BF16),
        ),
        in_specs=[pl.BlockSpec(memory_space=pl.ANY)] * len(operands),
        out_specs=(pl.BlockSpec(memory_space=pltpu.VMEM),) * 3,
        scratch_shapes=scratch,
        compiler_params=pltpu.CompilerParams(
            collective_id=0, has_side_effects=True, vmem_limit_bytes=67043328
        ),
    )(*operands)


def solution(mesh):
    placed = (
        P("tp", "kv"),
        P(),
        P("kv", "tp"),
        P("kv", "tp"),
        P("kv", None),
        P(),
        P(),
        P(None, "tp", None),
        P(None, "tp", None),
        P("tp", "kv"),
        P(),
        P(),
        P("kv", "tp"),
        P("kv", "tp"),
        P("tp", "kv"),
        P("tp", "kv", None),
        P("tp", "kv", None),
    )
    return jax.shard_map(
        body,
        mesh=mesh,
        in_specs=placed,
        out_specs=(P("tp", "kv"), P("tp", None), P("tp", None)),
        check_vma=False,
    )
```

time: 411 us -> 120 us (0.29)
  waiting for transfers between devices: 175 us -> 0 us
  Pallas kernels: 0 us -> 113 us
  blocking collectives: 91.5 us -> 0 us
  starting transfers between devices: 91.1 us -> 0 us
  between operations: 14.6 us -> 0.64 us
  local copies, waits for them, and re-layouts: 18.3 us -> 5.63 us
  other arithmetic: 12.6 us -> 0 us
  matrix products: 6.91 us -> 0 us
    pallas_call x0 -> x1, Pallas kernels: none -> 113 us  [body(): pl.pallas_call(functools.partial(kernel, n_kv, n_tp), out_shape=(jax.Shap...]
    all_to_all x11 -> x0, waiting for transfers between devices: 100 us -> none  [the longest x7 53.1 us: sent_to_all(): lax.all_to_all(jnp.broadcast_to(array[None], (size, *array.shape)), axis,...]
    all_to_all x11 -> x0, starting transfers between devices: 91.1 us -> none  [the longest x7 47.6 us: sent_to_all(): lax.all_to_all(jnp.broadcast_to(array[None], (size, *array.shape)), axis,...]
    unnamed x2 -> x0, waiting for transfers between devices: 74.4 us -> none
    all_to_all x3 -> x0, blocking collectives: 47.5 us -> none  [the longest x2 29.7 us: sent_to_all(): lax.all_to_all(jnp.broadcast_to(array[None], (size, *array.shape)), axis,...]
    psum x4 -> x0, blocking collectives: 30.3 us -> none  [by_axis(): return functools.reduce(lax.psum, axes, array)]
    pmax x2 -> x0, blocking collectives: 13.7 us -> none  [over_axes(): return functools.reduce(lax.pmax, axes, array)]
    dot_general x15 -> x0, matrix products: 6.91 us -> none  [the longest x1 1.13 us: body(): gate_part = jnp.dot(normed_m, w_gate, preferred_element_type=jnp.float32)]
  transfers between devices with their start and end apart: 12 -> 0, of which waited for: 11 -> 0; matrix products, arithmetic and copies ran while one was open for 4% -> 0% of each run, Pallas kernels for 0% -> 0%
where the time goes in v1:
time: 120 us; the launch traced here: 119 us
  Pallas kernels  113 us (94%)
  local copies, waits for them, and re-layouts  5.63 us (5%)
    pallas_call x1, Pallas kernels, body(): pl.pallas_call(functools.partial(kernel, n_kv, n_tp), out_shape=(jax.Shap...  113 us
    unnamed x3, local copies, waits for them, and re-layouts  3.75 us

profile of v1, /device:TPU:1, one launch (start us, length us, event | category | flops | bytes accessed | tf_op | source)
XLA Modules:
  0.0 119.5 jit_solution(11283935494941332088)
XLA Ops:
  0.6 1.9 %copy_bitcast_fusion = (bf16[2,512,128]{2,1,0:T(8,128)(2,1)}, bf16[2,512,128]{2,1,0:T(8,128)(2,1)}) fusion(bf16[512,2,128]{2,1,0:T(2,128)(2,1)} %param.26, bf16[512,2,128]{2,1,0:T(2,128)(2,1)} %param.25), kind=kLoop, calls=%fused_computation | loop fusion | bytes 1048576 | tf_op jit(solution)/shard_map/transpose | solution.py:430
  2.5 113.2 %shard_map.193 = (bf16[4,256]{1,0:T(4,128)(2,1)}, bf16[4,512]{1,0:T(4,128)(2,1)}, bf16[4,64]{1,0:T(4,128)(2,1)}) custom-call(bf16[4,256]{1,0:T(4,128)(2,1)} %refs_0_.1, bf16[32,128]{1,0:T(8,128)(2,1)} %bitcast.16, bf16[32,128]{1,0:T(8,128)(2,1)} %bitcast.17, bf16[32,128]{1,0:T(8,128)(2,1)} %bitcast.18, bf16[4,128]{1,0:T(4,128)(2,1)} %bitcast.19, ...), custom_call_target="tpu_custom_call" | custom-call | tf_op jit(solution)/shard_map/pallas_call | solution.py:486
  115.7 1.2 %copy.28 = bf16[4,256]{1,0:T(4,128)(2,1)} copy(bf16[4,256]{1,0:T(4,128)(2,1)} %get-tuple-element.8) | data formatting | bytes 4096
  117.0 1.3 %copy.29 = bf16[4,512]{1,0:T(4,128)(2,1)} copy(bf16[4,512]{1,0:T(4,128)(2,1)} %get-tuple-element.9) | data formatting | bytes 8192
  118.3 1.2 %copy.30 = bf16[4,64]{1,0:T(4,128)(2,1)} copy(bf16[4,64]{1,0:T(4,128)(2,1)} %get-tuple-element.10) | data formatting | bytes 1024

commit v2 on v1

--- a/solution.py
+++ b/solution.py
@@ -79,13 +79,13 @@
 def kernel(n_kv, n_tp, *refs):
     n_in = len(INPUTS)
     hbm = dict(zip(INPUTS, refs[:n_in]))
-    out_resid, out_latent, out_key = refs[n_in : n_in + 3]
-    scratch = refs[n_in + 3 :]
+    out = refs[n_in]
+    scratch = refs[n_in + 1 :]
     v = dict(zip(INPUTS, scratch[:n_in]))
     (
         load_sem,
         f1, sb_l, rb_l, rb1, f2, sb2, rb2, f3, sb3, rb3, fq, rb_q, sb4, rb4, f5, sb5, rb5, fo, rb6,
-        f7, sb7, rb7, sb8, rb8, mid, rb9, f10, sb10, rb10, sb11, rb11, rb12, sb12, g1, nl,
+        f7, sb7, rb7, sb8, rb8, mid, rb9, f10, sb10, rb10, sb11, rb11, rb12, sb12, g1, nl, pairs, up_k, up_v,
         tp_send, tp_recv, kv_send, kv_recv, q_recv, o_recv,
     ) = scratch[n_in:]
 
@@ -101,8 +101,25 @@
     heads_q = heads // quarters
     tp_q = n_tp // quarters
     ff = v["wg"].shape[0]
-    scale = (v["ku"].shape[2] + 64) ** (-0.5)
+    scale = (128 + 64) ** (-0.5)
     slot, group = lax.rem(k, own), lax.div(k, own)
+
+    def far_tp(i):
+        return lax.rem(t + n_tp // 2 + lax.div(i + 1, 2) * (1 - 2 * lax.rem(i, 2)) + n_tp, n_tp)
+
+    rows_kv = n_kv // own
+    steps = [(y, x) for y in range(rows_kv) for x in range(own) if (y, x) != (0, 0)]
+    steps.sort(key=lambda step: -min(step[0], rows_kv - step[0]) - min(step[1], own - step[1]))
+    far_kv = [lax.rem(group + y, rows_kv) * own + lax.rem(slot + x, own) for y, x in steps]
+
+    barrier = pltpu.get_barrier_semaphore()
+
+    @pl.loop(0, n_tp - 1)
+    def _(i):
+        pl.semaphore_signal(barrier, inc=1, device_id={"kv": k, "tp": far_tp(i)}, device_id_type=MESH)
+
+    for to in far_kv:
+        pl.semaphore_signal(barrier, inc=1, device_id={"kv": to, "tp": t}, device_id_type=MESH)
 
     loads = {}
     for at, name in enumerate(INPUTS):
@@ -111,16 +128,6 @@
             source = source.at[:, pl.ds(pl.multiple_of(k * width, width), width)]
         loads[name] = pltpu.make_async_copy(source, v[name], load_sem.at[at])
         loads[name].start()
-
-    barrier = pltpu.get_barrier_semaphore()
-
-    @pl.loop(1, n_tp)
-    def _(i):
-        pl.semaphore_signal(barrier, inc=1, device_id={"kv": k, "tp": lax.rem(t + i, n_tp)}, device_id_type=MESH)
-
-    @pl.loop(1, n_kv)
-    def _(i):
-        pl.semaphore_signal(barrier, inc=1, device_id={"kv": lax.rem(k + i, n_kv), "tp": t}, device_id_type=MESH)
 
     def send(src, dst, send_sem, recv_sem, kv, tp):
         pltpu.make_async_remote_copy(
@@ -133,16 +140,22 @@
         ).start()
 
     def over_tp(src_of, dst, phase):
-        @pl.loop(1, n_tp)
+        @pl.loop(0, n_tp - 1)
         def _(i):
-            to = lax.rem(t + i, n_tp)
+            to = far_tp(i)
             send(src_of(to), dst, tp_send.at[phase], tp_recv.at[phase], k, to)
 
     def over_kv(src_of, dst, phase, recv=None):
-        @pl.loop(1, n_kv)
-        def _(i):
-            to = lax.rem(k + i, n_kv)
+        for to in far_kv:
             send(src_of(to), dst, kv_send.at[phase], kv_recv.at[phase] if recv is None else recv, to, t)
+
+    def by_head(name, to):
+        @pl.loop(0, lat, unroll=16)
+        def _(c):
+            pairs[pl.ds(2 * c, 2), :] = v[name][c].astype(F32)
+
+        for h in range(2):
+            to[h] = pairs[pl.ds(h, lat, stride=2), :].astype(BF16)
 
     def take(ref, sem):
         pltpu.make_async_copy(ref, ref, sem).wait()
@@ -178,6 +191,7 @@
     for name in INPUTS:
         if name in ("wqn", "wqr", "ku", "vu", "wo", "wg", "wu", "wd"):
             loads[name].wait()
+    by_head("ku", up_k)
     take_tp(rb1, 0)
     for j in range(n_tp):
         f1[own * j : own * (j + 1), :] = rb1[j].astype(F32)
@@ -204,12 +218,12 @@
     new_latent = (
         latent * lax.rsqrt(jnp.mean(latent * latent, axis=1, keepdims=True) + EPS) * latent_gain
     ).astype(BF16)
-    out_latent[...] = new_latent
+    out[:, width : width + lat] = new_latent.astype(F32)
     key = total[:, lat : lat + 128]
     own_scale = lax.rsqrt(key[:, 64:65] / model + EPS)
     table = v["table"][...]
     new_key = rotate(key * own_scale, table).astype(BF16)
-    out_key[...] = new_key[:, 0:64]
+    out[:, width + lat : width + lat + 128] = new_key.astype(F32)
     nl[:, 0:lat] = new_latent.astype(F32)
     nl[:, lat : lat + 128] = jnp.where(lanes((own, 128)) < 64, new_key.astype(F32), 0.0)
 
@@ -223,7 +237,7 @@
     q_rope = rotate(total[:, qw : qw + 128] * scale_in, table)
     for h in range(2):
         spot = pl.ds(h, share, stride=2)
-        put(f3, spot, dot(q_nope[:, 128 * h : 128 * (h + 1)], v["ku"][h], NT))
+        put(f3, spot, dot(q_nope[:, 128 * h : 128 * (h + 1)], up_k[h], NT))
         turned = q_rope if h == 0 else pltpu.roll(q_rope, 64, 1)
         put(f3, spot, jnp.where(lanes((share, 128)) < 64, turned, 0.0), lat // 128)
     for i in range(share):
@@ -240,6 +254,7 @@
         def _():
             rb3[t] = sb3[i]
 
+    by_head("vu", up_v)
     gathers_q = lax.rem(t, quarters) == group
 
     @pl.when(gathers_q)
@@ -319,7 +334,7 @@
         take_tp(rb5, 2)
         for j in range(n_tp):
             put(fo, slice(2 * j, 2 * j + 2), rb5[j].astype(F32))
-        terms = [dot(get(fo, pl.ds(h, n_tp, stride=2)).astype(BF16), v["vu"][h]).astype(BF16) for h in range(2)]
+        terms = [dot(get(fo, pl.ds(h, n_tp, stride=2)).astype(BF16), up_v[h]).astype(BF16) for h in range(2)]
         rb6[slot] = jnp.concatenate(terms, axis=1)
         over_kv(lambda to: rb6.at[slot], rb6.at[slot], 4, o_recv.at[slot])
 
@@ -378,7 +393,7 @@
     over_tp(lambda to: sb12.at[to], rb12.at[t], 5)
     rb12[t] = sb12[t]
     take_tp(rb12, 5)
-    out_resid[...] = (mid[...].astype(F32) + jnp.sum(rb12[...].astype(F32), axis=0)).astype(BF16)
+    out[:, 0:width] = mid[...].astype(F32) + jnp.sum(rb12[...].astype(F32), axis=0)
 
     for phase, ref in ((0, rb1), (3, rb7), (4, rb9), (5, rb12)):
         take(ref.at[pl.ds(0, n_tp - 1)], tp_send.at[phase])
@@ -399,6 +414,11 @@
             @pl.loop(1, n_kv)
             def _(i):
                 take(ref.at[0], kv_send.at[phase])
+
+
+def split(parts, whole, *outs):
+    for (start, size), out in zip(parts, outs):
+        out[...] = whole[:, start : start + size].astype(BF16)
 
 
 def body(
@@ -426,8 +446,8 @@
         w_query_rope,
         w_latent,
         w_key_rope.T,
-        key_up.transpose(1, 0, 2),
-        value_up.transpose(1, 0, 2),
+        key_up,
+        value_up,
         w_out,
         w_gate.T,
         w_up.T,
@@ -476,6 +496,9 @@
         pltpu.VMEM((n_tp, own, width), BF16),
         pltpu.VMEM((attn_gain.shape[0] // 128, 128), F32),
         pltpu.VMEM((own, wide), F32),
+        pltpu.VMEM((2 * lat, 128), F32),
+        pltpu.VMEM((2, lat, 128), BF16),
+        pltpu.VMEM((2, lat, 128), BF16),
         dma((6,)),
         dma((6,)),
         dma((8,)),
@@ -483,20 +506,23 @@
         dma((own,)),
         dma((own,)),
     ]
-    return pl.pallas_call(
+    out = pl.pallas_call(
         functools.partial(kernel, n_kv, n_tp),
-        out_shape=(
-            jax.ShapeDtypeStruct((own, width), BF16),
-            jax.ShapeDtypeStruct((own, lat), BF16),
-            jax.ShapeDtypeStruct((own, 64), BF16),
-        ),
+        out_shape=jax.ShapeDtypeStruct((own, width + wide), F32),
         in_specs=[pl.BlockSpec(memory_space=pl.ANY)] * len(operands),
-        out_specs=(pl.BlockSpec(memory_space=pltpu.VMEM),) * 3,
+        out_specs=pl.BlockSpec(memory_space=pltpu.VMEM),
         scratch_shapes=scratch,
         compiler_params=pltpu.CompilerParams(
             collective_id=0, has_side_effects=True, vmem_limit_bytes=67043328
         ),
     )(*operands)
+    parts = ((0, width), (width, lat), (width + lat, 64))
+    return pl.pallas_call(
+        functools.partial(split, parts),
+        out_shape=tuple(jax.ShapeDtypeStruct((own, size), BF16) for _, size in parts),
+        in_specs=[pl.BlockSpec(memory_space=pltpu.VMEM)],
+        out_specs=(pl.BlockSpec(memory_space=pltpu.VMEM),) * 3,
+    )(out)
 
 
 def solution(mesh):

time: 120 us -> 109 us (0.908)
  local copies, waits for them, and re-layouts: 5.63 us -> 0 us
  Pallas kernels: 113 us -> 108 us
    pallas_call x1 -> x2, Pallas kernels: 113 us -> 108 us  [the longest x1 107 us: body(): pl.pallas_call(functools.partial(kernel, n_kv, n_tp), out_shape=jax.Shape...]
    unnamed x3 -> x0, local copies, waits for them, and re-layouts: 3.75 us -> none
    transpose x1 -> x0, local copies, waits for them, and re-layouts: 1.88 us -> none  [body(): value_up.transpose(1, 0, 2)]
where the time goes in v2:
time: 109 us
  Pallas kernels  108 us (99%)
    pallas_call x1, Pallas kernels, body(): pl.pallas_call(functools.partial(kernel, n_kv, n_tp), out_shape=jax.Shape...  107 us

profile of v2, /device:TPU:1, one launch (start us, length us, event | category | flops | bytes accessed | tf_op | source)
XLA Modules:
  0.0 108.8 jit_solution(14168002111637940773)
XLA Ops:
  0.6 106.9 %shard_map.193.whole = f32[4,896]{1,0:T(4,128)} custom-call(bf16[4,256]{1,0:T(4,128)(2,1)} %refs_0_.1, bf16[32,128]{1,0:T(8,128)(2,1)} %bitcast.12, bf16[32,128]{1,0:T(8,128)(2,1)} %bitcast.13, bf16[32,128]{1,0:T(8,128)(2,1)} %bitcast.14, bf16[4,128]{1,0:T(4,128)(2,1)} %bitcast.15, f32[2,128]{1,0:T(2,128)} %constant.2.clone.refs_5_, ...), custom_call_target="tpu_custom_call" | custom-call | tf_op jit(solution)/shard_map/pallas_call | solution.py:509
  107.5 1.3 %shard_map.194 = (bf16[4,256]{1,0:T(4,128)(2,1)}, bf16[4,512]{1,0:T(4,128)(2,1)}, bf16[4,64]{1,0:T(4,128)(2,1)}) custom-call(f32[4,896]{1,0:T(4,128)} %shard_map.193.whole), custom_call_target="tpu_custom_call" | custom-call | tf_op jit(solution)/shard_map/pallas_call | solution.py:520

commit v3 on v2

--- a/solution.py
+++ b/solution.py
@@ -85,7 +85,7 @@
     (
         load_sem,
         f1, sb_l, rb_l, rb1, f2, sb2, rb2, f3, sb3, rb3, fq, rb_q, sb4, rb4, f5, sb5, rb5, fo, rb6,
-        f7, sb7, rb7, sb8, rb8, mid, rb9, f10, sb10, rb10, sb11, rb11, rb12, sb12, g1, nl, pairs, up_k, up_v,
+        f7, sb7, rb7, sb8, rb8, mid, rb9, f10, sb10, rb10, sb_r, rb_r, sum_r, f2r, sb11, rb11, rb12, sb12, g1, nl, pairs, up_k, up_v,
         tp_send, tp_recv, kv_send, kv_recv, q_recv, o_recv,
     ) = scratch[n_in:]
 
@@ -102,22 +102,24 @@
     tp_q = n_tp // quarters
     ff = v["wg"].shape[0]
     scale = (128 + 64) ** (-0.5)
+    padded = -(-ff // 128) * 128
+    free = padded - ff
+    lane_row = lanes((batch, 128))
     slot, group = lax.rem(k, own), lax.div(k, own)
 
-    def far_tp(i):
-        return lax.rem(t + n_tp // 2 + lax.div(i + 1, 2) * (1 - 2 * lax.rem(i, 2)) + n_tp, n_tp)
-
+    around = [n_tp // 2 + (i + 1) // 2 * (1 - 2 * (i % 2)) for i in range(n_tp - 1)]
+    far_tp = [lax.rem(t + offset, n_tp) for offset in around]
     rows_kv = n_kv // own
     steps = [(y, x) for y in range(rows_kv) for x in range(own) if (y, x) != (0, 0)]
     steps.sort(key=lambda step: -min(step[0], rows_kv - step[0]) - min(step[1], own - step[1]))
     far_kv = [lax.rem(group + y, rows_kv) * own + lax.rem(slot + x, own) for y, x in steps]
 
+    first = pltpu.make_async_copy(hbm["resid"], v["resid"], load_sem.at[0])
+    first.start()
     barrier = pltpu.get_barrier_semaphore()
 
-    @pl.loop(0, n_tp - 1)
-    def _(i):
-        pl.semaphore_signal(barrier, inc=1, device_id={"kv": k, "tp": far_tp(i)}, device_id_type=MESH)
-
+    for to in far_tp:
+        pl.semaphore_signal(barrier, inc=1, device_id={"kv": k, "tp": to}, device_id_type=MESH)
     for to in far_kv:
         pl.semaphore_signal(barrier, inc=1, device_id={"kv": to, "tp": t}, device_id_type=MESH)
 
@@ -126,8 +128,9 @@
         source = hbm[name]
         if name == "wkr":
             source = source.at[:, pl.ds(pl.multiple_of(k * width, width), width)]
-        loads[name] = pltpu.make_async_copy(source, v[name], load_sem.at[at])
-        loads[name].start()
+        loads[name] = first if name == "resid" else pltpu.make_async_copy(source, v[name], load_sem.at[at])
+        if name != "resid":
+            loads[name].start()
 
     def send(src, dst, send_sem, recv_sem, kv, tp):
         pltpu.make_async_remote_copy(
@@ -140,9 +143,7 @@
         ).start()
 
     def over_tp(src_of, dst, phase):
-        @pl.loop(0, n_tp - 1)
-        def _(i):
-            to = far_tp(i)
+        for to in far_tp:
             send(src_of(to), dst, tp_send.at[phase], tp_recv.at[phase], k, to)
 
     def over_kv(src_of, dst, phase, recv=None):
@@ -157,6 +158,11 @@
         for h in range(2):
             to[h] = pairs[pl.ds(h, lat, stride=2), :].astype(BF16)
 
+    def gate_up(rows):
+        f10[:, 2 * padded - 128 : 2 * padded] = jnp.zeros((batch, 128), F32)
+        f10[:, 0:ff] = dot(rows, v["wg"][...], NT)
+        f10[:, padded : padded + ff] = dot(rows, v["wu"][...], NT)
+
     def take(ref, sem):
         pltpu.make_async_copy(ref, ref, sem).wait()
 
@@ -166,7 +172,12 @@
     def take_kv(ref, phase):
         take(ref.at[pl.ds(0, n_kv - 1)], kv_recv.at[phase])
 
-    for name in ("attn_gain", "post_gain", "mlp_gain", "resid", "wl", "wkr", "latent_gain", "table"):
+    first.wait()
+    pl.semaphore_wait(barrier, n_tp + n_kv - 2)
+
+    over_tp(lambda to: v["resid"], rb1.at[t], 0)
+    rb1[t] = v["resid"][...]
+    for name in ("attn_gain", "post_gain", "mlp_gain", "wl", "wkr", "latent_gain", "table"):
         loads[name].wait()
 
     def block_of(name):
@@ -181,12 +192,7 @@
     key_part = dot(own_normed, v["wkr"][...], NT)
     square = jnp.sum(resid * resid, axis=1, keepdims=True)
     sb_l[:, lat : lat + 128] = jnp.concatenate([key_part, jnp.broadcast_to(square, (own, 64))], axis=1)
-
-    pl.semaphore_wait(barrier, n_tp + n_kv - 2)
-
-    over_tp(lambda to: v["resid"], rb1.at[t], 0)
     over_kv(lambda to: sb_l, rb_l.at[k], 0)
-    rb1[t] = v["resid"][...]
     rb_l[k] = sb_l[...]
     for name in INPUTS:
         if name in ("wqn", "wqr", "ku", "vu", "wo", "wg", "wu", "wd"):
@@ -242,33 +248,57 @@
         put(f3, spot, jnp.where(lanes((share, 128)) < 64, turned, 0.0), lat // 128)
     for i in range(share):
         sb3[i] = get(f3, slice(2 * i, 2 * i + 2)).astype(BF16)
+    line = lax.div(t, tp_q)
+    place = lax.rem(t, tp_q)
+    stays = jnp.logical_and(line == group, lax.rem(t, quarters) == group)
+
     @pl.loop(0, share)
     def _(i):
         to = quarters * i + group
-
-        @pl.when(to != t)
-        def _():
-            send(sb3.at[i], rb3.at[t], tp_send.at[1], tp_recv.at[1], k, to)
-
-        @pl.when(to == t)
-        def _():
-            rb3[t] = sb3[i]
+        home = jnp.logical_and(to == t, line == group)
+
+        @pl.when(jnp.logical_not(home))
+        def _():
+            send(sb3.at[i], rb3.at[place], tp_send.at[1], tp_recv.at[1], own * line + slot, to)
+
+        @pl.when(home)
+        def _():
+            rb3[place] = sb3[i]
 
     by_head("vu", up_v)
-    gathers_q = lax.rem(t, quarters) == group
-
-    @pl.when(gathers_q)
+    normed = (f1[...] * mlp_gain).astype(BF16)
+    gate_up(normed)
+    f10[:, padded - 128 : padded] = jnp.where(
+        lane_row < 128 - free, f10[:, padded - 128 : padded], jnp.where(lane_row < 128 - free // 2, high, low)
+    )
+    for j in range(n_kv):
+        sb_r[j] = f10[share * j : share * (j + 1), :].astype(BF16)
+    over_kv(lambda to: sb_r.at[to], rb_r.at[k], 8)
+    rb_r[k] = sb_r[k]
+
+    @pl.when(stays)
     def _():
-        take_tp(rb3, 1)
-        for j in range(n_tp):
-            fq[2 * j : 2 * j + 2, :] = rb3[j].astype(F32)
-        rb_q[slot] = fq[...].astype(BF16)
-        over_kv(lambda to: rb_q.at[slot], rb_q.at[slot], 2, q_recv.at[slot])
+        take(rb3.at[pl.ds(0, tp_q - 1)], tp_recv.at[1])
+
+    @pl.when(jnp.logical_not(stays))
+    def _():
+        take(rb3, tp_recv.at[1])
+
+    for j in range(tp_q):
+        fq[2 * j : 2 * j + 2, :] = rb3[j].astype(F32)
+    part = pl.ds(pl.multiple_of(group * heads_q, heads_q), heads_q)
+    rb_q[slot, part, :] = fq[...].astype(BF16)
+    over_kv(lambda to: rb_q.at[slot, part], rb_q.at[slot, part], 2, q_recv.at[slot])
 
     loads["cl"].wait()
     loads["cr"].wait()
     for s in range(own):
-        @pl.when(k != own * lax.rem(t, quarters) + s)
+        @pl.when(slot == s)
+        def _():
+            if quarters > 1:
+                take(rb_q.at[s, pl.ds(0, heads_q * (quarters - 1))], q_recv.at[s])
+
+        @pl.when(slot != s)
         def _():
             take(rb_q.at[s], q_recv.at[s])
 
@@ -293,7 +323,7 @@
             def _():
                 rb4[k] = sb4[s, heads_q * q : heads_q * (q + 1), :]
 
-    query = rb_q[slot, pl.ds(pl.multiple_of(group * heads_q, heads_q), heads_q), :].astype(F32)
+    query = rb_q[slot, part, :].astype(F32)
     mine = nl[pl.ds(slot, 1), :]
     own_score = jnp.sum(query * mine, axis=1, keepdims=True) * scale
     take_kv(rb4, 3)
@@ -327,6 +357,11 @@
         def _():
             rb5[t] = sb5[i]
 
+    take_kv(rb_r, 8)
+    total = rb_r[0].astype(F32)
+    for j in range(1, n_kv):
+        total = total + rb_r[j].astype(F32)
+    sum_r[...] = total
     gathers_o = lax.div(t, tp_q) == group
 
     @pl.when(gathers_o)
@@ -353,23 +388,23 @@
     sb8[...] = jnp.broadcast_to(jnp.sum(attended * attended, axis=1, keepdims=True), sb8.shape)
     over_kv(lambda to: sb8, rb8.at[k], 5)
     rb8[k] = sb8[...]
-    take_kv(rb8, 5)
-    post_square = jnp.sum(rb8[...], axis=0)[:, 0:1]
-    mid[...] = (resid + attended * lax.rsqrt(post_square / model + EPS) * post_gain).astype(BF16)
+    mid[...] = attended.astype(BF16)
     over_tp(lambda to: mid, rb9.at[t], 4)
     rb9[t] = mid[...]
     take_tp(rb9, 4)
     for j in range(n_tp):
-        f1[own * j : own * (j + 1), :] = rb9[j].astype(F32)
-    rows = f1[...]
-    normed = (rows * mlp_gain).astype(BF16)
-    high, low = halves(jnp.sum(rows * rows, axis=1, keepdims=True))
-    padded = -(-ff // 128) * 128
-    free = padded - ff
-    f10[:, padded - 128 : padded] = jnp.where(lanes((batch, 128)) < 128 - free // 2, high, low)
-    f10[:, 2 * padded - 128 : 2 * padded] = jnp.zeros((batch, 128), F32)
-    f10[:, 0:ff] = dot(normed, v["wg"][...], NT)
-    f10[:, padded : padded + ff] = dot(normed, v["wu"][...], NT)
+        f2r[own * j : own * (j + 1), :] = rb9[j].astype(F32)
+    rows = f2r[...]
+    post = rows * post_gain
+    gate_up((post * mlp_gain).astype(BF16))
+    stats = []
+    for product in (rows * rows, f1[...] * post, post * post):
+        stats.extend(halves(jnp.sum(product, axis=1, keepdims=True)))
+    for at, picks in ((padded, stats[0:4]), (2 * padded, stats[4:6])):
+        tile = f10[:, at - 128 : at]
+        for n, pick in enumerate(picks):
+            tile = jnp.where(lane_row >= 128 - free + n * (free // len(picks)), pick, tile)
+        f10[:, at - 128 : at] = tile
     for j in range(n_kv):
         sb10[j] = f10[share * j : share * (j + 1), :].astype(BF16)
     over_kv(lambda to: sb10.at[to], rb10.at[k], 6)
@@ -378,9 +413,20 @@
     total = rb10[0].astype(F32)
     for j in range(1, n_kv):
         total = total + rb10[j].astype(F32)
-    squares = total[:, ff : ff + 1] + total[:, padded - 1 : padded]
-    scale_mid = lax.rsqrt(squares / model + EPS)
-    gate, up = total[:, 0:padded] * scale_mid, total[:, padded : 2 * padded] * scale_mid
+    base = sum_r[...]
+    quarter = free // 4
+
+    def stat(value, at, width):
+        return value[:, at : at + 1] + value[:, at + width : at + width + 1]
+
+    resid_square = stat(base, ff, free // 2)
+    factor = lax.rsqrt(stat(total, ff, quarter) / model + EPS)
+    mixed = stat(total, ff + 2 * quarter, quarter)
+    post_sum = stat(total, padded + ff, free // 2)
+    mid_square = jnp.maximum(resid_square + factor * (2.0 * mixed + factor * post_sum), 0.0)
+    scale_mid = lax.rsqrt(mid_square / model + EPS)
+    both = (base + factor * total) * scale_mid
+    gate, up = both[:, 0:padded], both[:, padded : 2 * padded]
     hidden = gate / (1.0 + jnp.exp(-gate)) * up
     sb11[...] = jnp.where(lanes((share, padded)) < ff, hidden, 0.0).astype(BF16)
     over_kv(lambda to: sb11, rb11.at[k], 7)
@@ -392,14 +438,17 @@
         sb12[j] = f1[own * j : own * (j + 1), :].astype(BF16)
     over_tp(lambda to: sb12.at[to], rb12.at[t], 5)
     rb12[t] = sb12[t]
+    take_kv(rb8, 5)
+    post_square = jnp.sum(rb8[...], axis=0)[:, 0:1]
+    resid_mid = (resid + attended * lax.rsqrt(post_square / model + EPS) * post_gain).astype(BF16).astype(F32)
     take_tp(rb12, 5)
-    out[:, 0:width] = mid[...].astype(F32) + jnp.sum(rb12[...].astype(F32), axis=0)
+    out[:, 0:width] = resid_mid + jnp.sum(rb12[...].astype(F32), axis=0)
 
     for phase, ref in ((0, rb1), (3, rb7), (4, rb9), (5, rb12)):
         take(ref.at[pl.ds(0, n_tp - 1)], tp_send.at[phase])
-    for phase, ref in ((0, rb_l), (1, rb2), (3, rb4), (5, rb8), (6, rb10), (7, rb11)):
+    for phase, ref in ((0, rb_l), (1, rb2), (3, rb4), (5, rb8), (6, rb10), (7, rb11), (8, rb_r)):
         take(ref.at[pl.ds(0, n_kv - 1)], kv_send.at[phase])
-    for phase, ref, count, inside in ((1, rb3, share, gathers_q), (2, rb5, tp_q, gathers_o)):
+    for phase, ref, count, inside in ((1, sb3, share, stays), (2, rb5, tp_q, gathers_o)):
         @pl.when(inside)
         def _():
             take(ref.at[pl.ds(0, count - 1)], tp_send.at[phase])
@@ -408,12 +457,13 @@
         def _():
             take(ref.at[pl.ds(0, count)], tp_send.at[phase])
 
-    for phase, ref, inside in ((2, rb_q, gathers_q), (4, rb6, gathers_o)):
-        @pl.when(inside)
-        def _():
-            @pl.loop(1, n_kv)
-            def _(i):
-                take(ref.at[0], kv_send.at[phase])
+    take(rb4.at[pl.ds(0, n_kv - 1)], kv_send.at[2])
+
+    @pl.when(gathers_o)
+    def _():
+        @pl.loop(1, n_kv)
+        def _(i):
+            take(rb6.at[0], kv_send.at[4])
 
 
 def split(parts, whole, *outs):
@@ -470,8 +520,8 @@
         pltpu.VMEM((n_kv, share, qw + 256), BF16),
         pltpu.VMEM((wide // 128, 2 * share, 128), F32),
         pltpu.VMEM((share, 2, wide), BF16),
-        pltpu.VMEM((n_tp, 2, wide), BF16),
-        pltpu.VMEM((heads, wide), F32),
+        pltpu.VMEM((tp_q, 2, wide), BF16),
+        pltpu.VMEM((heads_q, wide), F32),
         pltpu.VMEM((own, heads, wide), BF16),
         pltpu.VMEM((own, heads, wide), BF16),
         pltpu.VMEM((n_kv, heads_q, wide), BF16),
@@ -490,6 +540,10 @@
         pltpu.VMEM((batch, 2 * padded), F32),
         pltpu.VMEM((n_kv, share, 2 * padded), BF16),
         pltpu.VMEM((n_kv, share, 2 * padded), BF16),
+        pltpu.VMEM((n_kv, share, 2 * padded), BF16),
+        pltpu.VMEM((n_kv, share, 2 * padded), BF16),
+        pltpu.VMEM((share, 2 * padded), F32),
+        pltpu.VMEM((batch, width), F32),
         pltpu.VMEM((share, padded), BF16),
         pltpu.VMEM((n_kv, share, padded), BF16),
         pltpu.VMEM((n_tp, own, width), BF16),
@@ -501,8 +555,8 @@
         pltpu.VMEM((2, lat, 128), BF16),
         dma((6,)),
         dma((6,)),
-        dma((8,)),
-        dma((8,)),
+        dma((9,)),
+        dma((9,)),
         dma((own,)),
         dma((own,)),
     ]

time: 109 us -> 101 us (0.927)
  Pallas kernels: 108 us -> 99.7 us
    pallas_call x1, Pallas kernels: 107 us -> 98.4 us  [body(): pl.pallas_call(functools.partial(kernel, n_kv, n_tp), out_shape=jax.Shape...]
where the time goes in v3:
time: 101 us; the launch traced here: 100 us
  Pallas kernels  99.7 us (99%)
    pallas_call x1, Pallas kernels, body(): pl.pallas_call(functools.partial(kernel, n_kv, n_tp), out_shape=jax.Shape...  98.4 us

profile of v3, /device:TPU:1, one launch (start us, length us, event | category | flops | bytes accessed | tf_op | source)
XLA Modules:
  0.0 100.4 jit_solution(11415758616147181467)
XLA Ops:
  0.6 98.4 %shard_map.193.whole = f32[4,896]{1,0:T(4,128)} custom-call(bf16[4,256]{1,0:T(4,128)(2,1)} %refs_0_.1, bf16[32,128]{1,0:T(8,128)(2,1)} %bitcast.12, bf16[32,128]{1,0:T(8,128)(2,1)} %bitcast.13, bf16[32,128]{1,0:T(8,128)(2,1)} %bitcast.14, bf16[4,128]{1,0:T(4,128)(2,1)} %bitcast.15, f32[2,128]{1,0:T(2,128)} %constant.2.clone.refs_5_, ...), custom_call_target="tpu_custom_call" | custom-call | tf_op jit(solution)/shard_map/pallas_call | solution.py:563
  99.1 1.3 %shard_map.194 = (bf16[4,256]{1,0:T(4,128)(2,1)}, bf16[4,512]{1,0:T(4,128)(2,1)}, bf16[4,64]{1,0:T(4,128)(2,1)}) custom-call(f32[4,896]{1,0:T(4,128)} %shard_map.193.whole), custom_call_target="tpu_custom_call" | custom-call | tf_op jit(solution)/shard_map/pallas_call | solution.py:574

commit v4 on v3

--- a/solution.py
+++ b/solution.py
@@ -85,7 +85,7 @@
     (
         load_sem,
         f1, sb_l, rb_l, rb1, f2, sb2, rb2, f3, sb3, rb3, fq, rb_q, sb4, rb4, f5, sb5, rb5, fo, rb6,
-        f7, sb7, rb7, sb8, rb8, mid, rb9, f10, sb10, rb10, sb_r, rb_r, sum_r, f2r, sb11, rb11, rb12, sb12, g1, nl, pairs, up_k, up_v,
+        f7, sb7, rb7, sb8, rb8, mid, rb9, f10, sb10, rb10, sb_r, rb_r, sum_r, f2r, sb11, rb11, rb12, sb12, g1, nl, pairs, up_k, up_v, factors,
         tp_send, tp_recv, kv_send, kv_recv, q_recv, o_recv,
     ) = scratch[n_in:]
 
@@ -203,12 +203,10 @@
         f1[own * j : own * (j + 1), :] = rb1[j].astype(F32)
     rows = f1[...]
     normed = (rows * attn_gain).astype(BF16)
-    high, low = halves(jnp.sum(rows * rows, axis=1, keepdims=True))
     qw = v["wqn"].shape[1]
     every = slice(None)
     put(f2, every, dot(normed, v["wqn"][...]))
     put(f2, every, dot(normed, v["wqr"][...]), qw // 128)
-    put(f2, every, jnp.where(lanes((batch, 128)) < 64, high, low), qw // 128 + 1)
     for j in range(n_kv):
         sb2[j] = get(f2, pl.ds(j, share, stride=n_kv)).astype(BF16)
     over_kv(lambda to: sb2.at[to], rb2.at[k], 1)
@@ -230,6 +228,7 @@
     table = v["table"][...]
     new_key = rotate(key * own_scale, table).astype(BF16)
     out[:, width + lat : width + lat + 128] = new_key.astype(F32)
+    factors[...] = jnp.broadcast_to(own_scale * scale, factors.shape)
     nl[:, 0:lat] = new_latent.astype(F32)
     nl[:, lat : lat + 128] = jnp.where(lanes((own, 128)) < 64, new_key.astype(F32), 0.0)
 
@@ -237,10 +236,8 @@
     total = rb2[0].astype(F32)
     for j in range(1, n_kv):
         total = total + rb2[j].astype(F32)
-    squares = total[:, qw + 128 : qw + 129] + total[:, qw + 192 : qw + 193]
-    scale_in = lax.rsqrt(squares / model + EPS)
-    q_nope = (total[:, 0:qw] * scale_in).astype(BF16)
-    q_rope = rotate(total[:, qw : qw + 128] * scale_in, table)
+    q_nope = total[:, 0:qw].astype(BF16)
+    q_rope = rotate(total[:, qw : qw + 128], table)
     for h in range(2):
         spot = pl.ds(h, share, stride=2)
         put(f3, spot, dot(q_nope[:, 128 * h : 128 * (h + 1)], up_k[h], NT))
@@ -248,14 +245,13 @@
         put(f3, spot, jnp.where(lanes((share, 128)) < 64, turned, 0.0), lat // 128)
     for i in range(share):
         sb3[i] = get(f3, slice(2 * i, 2 * i + 2)).astype(BF16)
-    line = lax.div(t, tp_q)
-    place = lax.rem(t, tp_q)
-    stays = jnp.logical_and(line == group, lax.rem(t, quarters) == group)
+    line, place = lax.rem(t, quarters), lax.div(t, quarters)
+    stays = line == group
 
     @pl.loop(0, share)
     def _(i):
         to = quarters * i + group
-        home = jnp.logical_and(to == t, line == group)
+        home = to == t
 
         @pl.when(jnp.logical_not(home))
         def _():
@@ -266,6 +262,7 @@
             rb3[place] = sb3[i]
 
     by_head("vu", up_v)
+    high, low = halves(jnp.sum(rows * rows, axis=1, keepdims=True))
     normed = (f1[...] * mlp_gain).astype(BF16)
     gate_up(normed)
     f10[:, padded - 128 : padded] = jnp.where(
@@ -303,7 +300,7 @@
             take(rb_q.at[s], q_recv.at[s])
 
         keys = v["cl"][s]
-        scores = (dot(rb_q[s, :, 0:lat], keys, NT) + dot(rb_q[s, :, lat : lat + 64], v["cr"][s])) * scale
+        scores = (dot(rb_q[s, :, 0:lat], keys, NT) + dot(rb_q[s, :, lat : lat + 64], v["cr"][s])) * factors[s : s + 1, 0:1]
         peak_high, peak_low = halves(jnp.max(scores, axis=1, keepdims=True))
         probs = jnp.exp(scores - (peak_high + peak_low))
         sum_high, sum_low = halves(jnp.sum(probs, axis=1, keepdims=True))
@@ -325,7 +322,7 @@
 
     query = rb_q[slot, part, :].astype(F32)
     mine = nl[pl.ds(slot, 1), :]
-    own_score = jnp.sum(query * mine, axis=1, keepdims=True) * scale
+    own_score = jnp.sum(query * mine, axis=1, keepdims=True) * factors[pl.ds(slot, 1), :][:, 0:1]
     take_kv(rb4, 3)
     peaks, sums = [], []
     top = own_score
@@ -347,7 +344,7 @@
 
     @pl.loop(0, tp_q)
     def _(i):
-        to = tp_q * group + i
+        to = quarters * i + group
 
         @pl.when(to != t)
         def _():
@@ -362,7 +359,7 @@
     for j in range(1, n_kv):
         total = total + rb_r[j].astype(F32)
     sum_r[...] = total
-    gathers_o = lax.div(t, tp_q) == group
+    gathers_o = line == group
 
     @pl.when(gathers_o)
     def _():
@@ -374,7 +371,7 @@
         over_kv(lambda to: rb6.at[slot], rb6.at[slot], 4, o_recv.at[slot])
 
     for s in range(own):
-        @pl.when(k != own * lax.div(t, tp_q) + s)
+        @pl.when(k != own * line + s)
         def _():
             take(rb6.at[s], o_recv.at[s])
 
@@ -515,9 +512,9 @@
         pltpu.VMEM((own, wide), F32),
         pltpu.VMEM((n_kv, own, wide), F32),
         pltpu.VMEM((n_tp, own, width), BF16),
-        pltpu.VMEM((qw // 128 + 2, batch, 128), F32),
-        pltpu.VMEM((n_kv, share, qw + 256), BF16),
-        pltpu.VMEM((n_kv, share, qw + 256), BF16),
+        pltpu.VMEM((qw // 128 + 1, batch, 128), F32),
+        pltpu.VMEM((n_kv, share, qw + 128), BF16),
+        pltpu.VMEM((n_kv, share, qw + 128), BF16),
         pltpu.VMEM((wide // 128, 2 * share, 128), F32),
         pltpu.VMEM((share, 2, wide), BF16),
         pltpu.VMEM((tp_q, 2, wide), BF16),
@@ -553,6 +550,7 @@
         pltpu.VMEM((2 * lat, 128), F32),
         pltpu.VMEM((2, lat, 128), BF16),
         pltpu.VMEM((2, lat, 128), BF16),
+        pltpu.VMEM((own, 128), F32),
         dma((6,)),
         dma((6,)),
         dma((9,)),

time: 101 us -> 99.5 us (0.985)
    pallas_call x1, Pallas kernels: 98.4 us -> 97.3 us  [body(): pl.pallas_call(functools.partial(kernel, n_kv, n_tp), out_shape=jax.Shape...]
where the time goes in v4:
time: 99.5 us; the launch traced here: 99.3 us
  Pallas kernels  98.7 us (99%)
    pallas_call x1, Pallas kernels, body(): pl.pallas_call(functools.partial(kernel, n_kv, n_tp), out_shape=jax.Shape...  97.3 us

profile of v4, /device:TPU:1, one launch (start us, length us, event | category | flops | bytes accessed | tf_op | source)
XLA Modules:
  0.0 99.3 jit_solution(1887697889300286869)
XLA Ops:
  0.6 97.3 %shard_map.193.whole = f32[4,896]{1,0:T(4,128)} custom-call(bf16[4,256]{1,0:T(4,128)(2,1)} %refs_0_.1, bf16[32,128]{1,0:T(8,128)(2,1)} %bitcast.12, bf16[32,128]{1,0:T(8,128)(2,1)} %bitcast.13, bf16[32,128]{1,0:T(8,128)(2,1)} %bitcast.14, bf16[4,128]{1,0:T(4,128)(2,1)} %bitcast.15, f32[2,128]{1,0:T(2,128)} %constant.2.clone.refs_5_, ...), custom_call_target="tpu_custom_call" | custom-call | tf_op jit(solution)/shard_map/pallas_call | solution.py:561
  98.0 1.3 %shard_map.194 = (bf16[4,256]{1,0:T(4,128)(2,1)}, bf16[4,512]{1,0:T(4,128)(2,1)}, bf16[4,64]{1,0:T(4,128)(2,1)}) custom-call(f32[4,896]{1,0:T(4,128)} %shard_map.193.whole), custom_call_target="tpu_custom_call" | custom-call | tf_op jit(solution)/shard_map/pallas_call | solution.py:572

commit v5 on v4

--- a/solution.py
+++ b/solution.py
@@ -262,17 +262,6 @@
             rb3[place] = sb3[i]
 
     by_head("vu", up_v)
-    high, low = halves(jnp.sum(rows * rows, axis=1, keepdims=True))
-    normed = (f1[...] * mlp_gain).astype(BF16)
-    gate_up(normed)
-    f10[:, padded - 128 : padded] = jnp.where(
-        lane_row < 128 - free, f10[:, padded - 128 : padded], jnp.where(lane_row < 128 - free // 2, high, low)
-    )
-    for j in range(n_kv):
-        sb_r[j] = f10[share * j : share * (j + 1), :].astype(BF16)
-    over_kv(lambda to: sb_r.at[to], rb_r.at[k], 8)
-    rb_r[k] = sb_r[k]
-
     @pl.when(stays)
     def _():
         take(rb3.at[pl.ds(0, tp_q - 1)], tp_recv.at[1])
@@ -289,7 +278,7 @@
 
     loads["cl"].wait()
     loads["cr"].wait()
-    for s in range(own):
+    def scores_of(s):
         @pl.when(slot == s)
         def _():
             if quarters > 1:
@@ -299,12 +288,18 @@
         def _():
             take(rb_q.at[s], q_recv.at[s])
 
-        keys = v["cl"][s]
-        scores = (dot(rb_q[s, :, 0:lat], keys, NT) + dot(rb_q[s, :, lat : lat + 64], v["cr"][s])) * factors[s : s + 1, 0:1]
+        found = dot(rb_q[s, :, 0:lat], v["cl"][s], NT) + dot(rb_q[s, :, lat : lat + 64], v["cr"][s])
+        return found * factors[s : s + 1, 0:1]
+
+    following = scores_of(0)
+    for s in range(own):
+        scores = following
+        if s + 1 < own:
+            following = scores_of(s + 1)
         peak_high, peak_low = halves(jnp.max(scores, axis=1, keepdims=True))
         probs = jnp.exp(scores - (peak_high + peak_low))
         sum_high, sum_low = halves(jnp.sum(probs, axis=1, keepdims=True))
-        sb4[s, :, 0:lat] = dot(probs.astype(BF16), keys).astype(BF16)
+        sb4[s, :, 0:lat] = dot(probs.astype(BF16), v["cl"][s]).astype(BF16)
         lane = lanes((heads, 128))
         sb4[s, :, lat : lat + 128] = jnp.where(
             lane < 32, peak_high, jnp.where(lane < 64, peak_low, jnp.where(lane < 96, sum_high, sum_low))
@@ -354,11 +349,18 @@
         def _():
             rb5[t] = sb5[i]
 
-    take_kv(rb_r, 8)
-    total = rb_r[0].astype(F32)
-    for j in range(1, n_kv):
-        total = total + rb_r[j].astype(F32)
-    sum_r[...] = total
+    rows = f1[...]
+    high, low = halves(jnp.sum(rows * rows, axis=1, keepdims=True))
+    normed = (rows * mlp_gain).astype(BF16)
+    gate_up(normed)
+    f10[:, padded - 128 : padded] = jnp.where(
+        lane_row < 128 - free, f10[:, padded - 128 : padded], jnp.where(lane_row < 128 - free // 2, high, low)
+    )
+    for j in range(n_kv):
+        sb_r[j] = f10[share * j : share * (j + 1), :].astype(BF16)
+    over_kv(lambda to: sb_r.at[to], rb_r.at[k], 8)
+    rb_r[k] = sb_r[k]
+
     gathers_o = line == group
 
     @pl.when(gathers_o)
@@ -380,14 +382,19 @@
         sb7[j] = get(f7, pl.ds(j, own, stride=n_tp)).astype(BF16)
     over_tp(lambda to: sb7.at[to], rb7.at[t], 3)
     rb7[t] = sb7[t]
+    take_kv(rb_r, 8)
+    total = rb_r[0].astype(F32)
+    for j in range(1, n_kv):
+        total = total + rb_r[j].astype(F32)
+    sum_r[...] = total
     take_tp(rb7, 3)
     attended = jnp.sum(rb7[...].astype(F32), axis=0)
+    mid[...] = attended.astype(BF16)
+    over_tp(lambda to: mid, rb9.at[t], 4)
+    rb9[t] = mid[...]
     sb8[...] = jnp.broadcast_to(jnp.sum(attended * attended, axis=1, keepdims=True), sb8.shape)
     over_kv(lambda to: sb8, rb8.at[k], 5)
     rb8[k] = sb8[...]
-    mid[...] = attended.astype(BF16)
-    over_tp(lambda to: mid, rb9.at[t], 4)
-    rb9[t] = mid[...]
     take_tp(rb9, 4)
     for j in range(n_tp):
         f2r[own * j : own * (j + 1), :] = rb9[j].astype(F32)

time: 99.5 us -> 99.1 us (level)
  no operation moved by 1% of the time
where the time goes in v5:
time: 99.1 us; the launch traced here: 98.9 us
  Pallas kernels  98.2 us (99%)
    pallas_call x1, Pallas kernels, body(): pl.pallas_call(functools.partial(kernel, n_kv, n_tp), out_shape=jax.Shape...  96.9 us

profile of v5, /device:TPU:1, one launch (start us, length us, event | category | flops | bytes accessed | tf_op | source)
XLA Modules:
  0.0 98.9 jit_solution(3877082097378778002)
XLA Ops:
  0.6 96.9 %shard_map.193.whole = f32[4,896]{1,0:T(4,128)} custom-call(bf16[4,256]{1,0:T(4,128)(2,1)} %refs_0_.1, bf16[32,128]{1,0:T(8,128)(2,1)} %bitcast.12, bf16[32,128]{1,0:T(8,128)(2,1)} %bitcast.13, bf16[32,128]{1,0:T(8,128)(2,1)} %bitcast.14, bf16[4,128]{1,0:T(4,128)(2,1)} %bitcast.15, f32[2,128]{1,0:T(2,128)} %constant.2.clone.refs_5_, ...), custom_call_target="tpu_custom_call" | custom-call | tf_op jit(solution)/shard_map/pallas_call | solution.py:568
  97.5 1.3 %shard_map.194 = (bf16[4,256]{1,0:T(4,128)(2,1)}, bf16[4,512]{1,0:T(4,128)(2,1)}, bf16[4,64]{1,0:T(4,128)(2,1)}) custom-call(f32[4,896]{1,0:T(4,128)} %shard_map.193.whole), custom_call_target="tpu_custom_call" | custom-call | tf_op jit(solution)/shard_map/pallas_call | solution.py:579
